TPU v7x, 32 devices: a whole 2x2x4 slice. The times are simulated.
32 devices in a mesh: ep: 16 (over z, y, x), tp: 2 (over core).
Axes of the slice: x: 2, y: 2, z: 4, core: 2. Of those that a mesh axis runs over, the one named last changes fastest.
Arguments:
- tokens_in: bfloat16 [512, 2048], P('ep'), may hold values from -6 to 6
- state_in: float32 [512, 8, 64, 64], P('ep', 'tp'), may hold values from -4 to 4
- norm_mix: bfloat16 [2048], replicated, may hold values from 0.099609375 to 1.8984375
- w_recept: bfloat16 [2048, 512], P(None, 'tp'), may hold values from -0.125 to 0.125
- w_key: bfloat16 [2048, 512], P(None, 'tp'), may hold values from -0.125 to 0.125
- w_value: bfloat16 [2048, 512], P(None, 'tp'), may hold values from -0.125 to 0.125
- decay_down: bfloat16 [2048, 64], replicated, may hold values from -0.125 to 0.125
- decay_up: bfloat16 [64, 512], P(None, 'tp'), may hold values from -0.75 to 0.75
- decay_base: float32 [512], P('tp'), may hold values from -4 to 2
- iclr_down: bfloat16 [2048, 64], replicated, may hold values from -0.125 to 0.125
- iclr_up: bfloat16 [64, 512], P(None, 'tp'), may hold values from -0.75 to 0.75
- iclr_base: float32 [512], P('tp'), may hold values from -4 to 4
- key_scale: bfloat16 [512], P('tp'), may hold values from 0.099609375 to 1.8984375
- key_mix: bfloat16 [512], P('tp'), may hold values from 0.099609375 to 1.8984375
- w_out: bfloat16 [512, 2048], P('tp'), may hold values from -0.046875 to 0.046875
- norm_moe: bfloat16 [2048], replicated, may hold values from 0.099609375 to 1.8984375
- router_group: bfloat16 [2048, 2], replicated, may hold values from -0.125 to 0.125
- router_expert: bfloat16 [2048, 16], replicated, may hold values from -0.125 to 0.125
- routes: int32 [512, 4], P('ep'), may hold values from 0 to 15, as said below
- expert_gate: bfloat16 [16, 2048, 256], P('ep', None, 'tp'), may hold values from -0.125 to 0.125
- expert_up: bfloat16 [16, 2048, 256], P('ep', None, 'tp'), may hold values from -0.125 to 0.125
- expert_down: bfloat16 [16, 256, 2048], P('ep', 'tp'), may hold values from -1.5 to 1.5
Outputs:
- layer_out: bfloat16 [512, 2048], P('ep', 'tp')
- state_out: float32 [512, 8, 64, 64], P('ep', 'tp')
Inputs may be any that keep to these rules, and one draw needn't show every extreme that they name: `routes`: each row names 4 different experts of one group (the same value of id // 8). Among the rows of one device no expert is named by more than 16 rows, and in every draw one expert is named by exactly 16 rows of every device.
All inputs are finite; a program needn't handle non-finite values.
Results may differ from a plain program's by a relative error of at most 0.018.
Values may be sent and summed in bfloat16 or wider, within the bound.
A program may use at most 64 MiB of HBM per device.

v0:
```python
import functools

import jax
import jax.numpy as jnp
from jax import lax
from jax.experimental import pallas as pl
from jax.experimental.pallas import tpu as pltpu
from jax.sharding import PartitionSpec as P


def mixer_kernel(
    tokens_ref,
    norm_ref,
    w_recept_hbm,
    w_key_hbm,
    w_value_hbm,
    decay_down_ref,
    decay_up_ref,
    decay_base_ref,
    iclr_down_ref,
    iclr_up_ref,
    iclr_base_ref,
    key_scale_ref,
    key_mix_ref,
    state_hbm,
    mixed_ref,
    state_out_hbm,
    weights,
    state_buf,
    out_buf,
    vectors,
    value_t,
    mixed_t,
    weight_sems,
    in_sems,
    out_sems,
):
    f32 = jnp.float32
    bf16 = jnp.bfloat16
    seq_count, width = tokens_ref.shape
    heads, head_size = state_hbm.shape[1], state_hbm.shape[3]
    channels = heads * head_size
    n_chunks = in_sems.shape[0]
    per_chunk = seq_count // n_chunks
    rows_dims = (((1,), (1,)), ((), ()))
    weight_loads = [
        pltpu.make_async_copy(source, weights.at[index], weight_sems.at[index])
        for index, source in enumerate((w_key_hbm, w_value_hbm, w_recept_hbm))
    ]
    for load in weight_loads:
        load.start()
    state_loads = []
    state_stores = []
    for index in range(n_chunks):
        span = pl.ds(index * per_chunk, per_chunk)
        state_loads.append(
            pltpu.make_async_copy(state_hbm.at[span], state_buf.at[span], in_sems.at[index])
        )
        state_stores.append(
            pltpu.make_async_copy(out_buf.at[span], state_out_hbm.at[span], out_sems.at[index])
        )
        state_loads[index].start()

    tokens = tokens_ref[...].astype(f32)
    factor = lax.rsqrt(jnp.mean(tokens * tokens, axis=1, keepdims=True) + 1e-06)
    normed = (tokens * factor * norm_ref[...].reshape(1, width).astype(f32)).astype(bf16)
    decay_low = jnp.tanh(
        lax.dot_general(normed, decay_down_ref[...], rows_dims, preferred_element_type=f32)
    ).astype(bf16)
    iclr_low = lax.dot_general(
        normed, iclr_down_ref[...], rows_dims, preferred_element_type=f32
    ).astype(bf16)
    decay_in = decay_base_ref[...].reshape(1, channels) + jnp.dot(
        decay_low, decay_up_ref[...], preferred_element_type=f32
    )
    decays = jnp.exp(-jnp.exp(jnp.float32(-0.5)) * jax.nn.sigmoid(decay_in))
    rate = jax.nn.sigmoid(
        iclr_base_ref[...].reshape(1, channels)
        + jnp.dot(iclr_low, iclr_up_ref[...], preferred_element_type=f32)
    )
    projected = []
    for index in range(3):
        weight_loads[index].wait()
        rows = jnp.dot(normed, weights[index], preferred_element_type=f32)
        projected.append(rows.astype(bf16).astype(f32))
    key, value, recept = projected
    value_t[...] = value.T
    scaled = key * key_scale_ref[...].reshape(1, channels).astype(f32)
    key_mod = key * (1.0 + (rate - 1.0) * key_mix_ref[...].reshape(1, channels).astype(f32))
    for head in range(heads):
        span = slice(head * head_size, (head + 1) * head_size)
        part = scaled[:, span]
        unit = part * lax.rsqrt(jnp.sum(part * part, axis=1, keepdims=True) + 1e-06)
        vectors[0, head] = decays[:, span]
        vectors[1, head] = unit
        vectors[2, head] = unit * rate[:, span]
        vectors[3, head] = key_mod[:, span]
        vectors[4, head] = recept[:, span]

    lanes = lax.broadcasted_iota(jnp.int32, (head_size, seq_count), 1)

    def update(seq, carry):
        here = lanes == seq
        for head in range(heads):
            span = slice(head * head_size, (head + 1) * head_size)
            row = pl.ds(seq, 1)
            state = state_buf[seq, head]
            removed = jnp.sum(state * vectors[1, head, row, :], axis=1, keepdims=True)
            column = jnp.sum(jnp.where(here, value_t[span, :], 0.0), axis=1, keepdims=True)
            state = (
                state * vectors[0, head, row, :]
                - removed * vectors[2, head, row, :]
                + column * vectors[3, head, row, :]
            )
            out_buf[seq, head] = state
            mixed = jnp.sum(state * vectors[4, head, row, :], axis=1, keepdims=True)
            mixed_t[span, :] = jnp.where(here, mixed, mixed_t[span, :])
        return carry

    mixed_t[...] = jnp.zeros_like(mixed_t)
    for index in range(n_chunks):
        state_loads[index].wait()
        lax.fori_loop(index * per_chunk, (index + 1) * per_chunk, update, 0, unroll=2)
        state_stores[index].start()
    mixed_ref[...] = mixed_t[...].T.astype(bf16)
    for store in state_stores:
        store.wait()


def moe_kernel(
    ep_count,
    block_rows,
    mixed_ref,
    w_out_hbm,
    tokens_ref,
    norm_ref,
    router_group_ref,
    router_expert_ref,
    routes_ref,
    gate_hbm,
    up_hbm,
    down_hbm,
    moe_ref,
    mid_ref,
    gate_ref,
    up_ref,
    down_ref,
    w_out_ref,
    part_buf,
    part_recv,
    mid_buf,
    norm_buf,
    send_buf,
    rows_buf,
    hidden_buf,
    term_send,
    term_own,
    term_recv,
    result_buf,
    back_buf,
    part_sems,
    out_send_sems,
    out_recv_sems,
    pair_send_sems,
    pair_recv_sems,
    term_send_sems,
    term_recv_sems,
    back_send_sems,
    back_recv_sems,
    load_sems,
):
    f32 = jnp.float32
    bf16 = jnp.bfloat16
    me = lax.axis_index("ep")
    core = lax.axis_index("tp")
    other = 1 - core
    seq_count, width = tokens_ref.shape
    half = width // 2
    cap = send_buf.shape[1]
    total_rows = ep_count * cap
    per_block = block_rows // cap
    n_blocks = total_rows // block_rows
    mesh_ids = pl.DeviceIdType.MESH

    def peer_at(step):
        return lax.rem(me + step, ep_count)

    def step_at(index):
        return 1 + lax.rem(index + ep_count // 2 - 1, ep_count - 1)

    barrier = pltpu.get_barrier_semaphore()
    pl.semaphore_signal(barrier, inc=1, device_id=(me, other), device_id_type=mesh_ids)

    def greet(step, carry):
        pl.semaphore_signal(
            barrier, inc=1, device_id=(peer_at(step), core), device_id_type=mesh_ids
        )
        return carry

    lax.fori_loop(1, ep_count, greet, 0)

    loads = [
        pltpu.make_async_copy(w_out_hbm, w_out_ref, load_sems.at[0]),
        pltpu.make_async_copy(gate_hbm.at[0], gate_ref, load_sems.at[1]),
        pltpu.make_async_copy(up_hbm.at[0], up_ref, load_sems.at[2]),
        pltpu.make_async_copy(down_hbm.at[0, :, pl.ds(0, half)], down_ref.at[0], load_sems.at[3]),
        pltpu.make_async_copy(down_hbm.at[0, :, pl.ds(half, half)], down_ref.at[1], load_sems.at[4]),
    ]
    for load in loads:
        load.start()

    n_groups = router_group_ref.shape[0]
    expert_ids = lax.broadcasted_iota(jnp.int32, (ep_count, seq_count), 0)
    uses = jnp.zeros((ep_count, seq_count), f32)
    for index in range(routes_ref.shape[0]):
        uses += jnp.where(routes_ref[index : index + 1, :] == expert_ids, 1.0, 0.0)
    group_ids = lax.broadcasted_iota(jnp.int32, (n_groups, seq_count), 0)
    group_hit = jnp.where(
        routes_ref[0:1, :] // (ep_count // n_groups) == group_ids, 1.0, 0.0
    )
    row_ids = lax.broadcasted_iota(jnp.int32, (seq_count, seq_count), 0)
    column_ids = lax.broadcasted_iota(jnp.int32, (seq_count, seq_count), 1)
    earlier = jnp.where(row_ids < column_ids, 1.0, 0.0).astype(bf16)
    position = jnp.dot(uses.astype(bf16), earlier, preferred_element_type=f32)
    slots = jnp.where(uses > 0.5, position, -1.0).astype(bf16)
    slot_rows = lax.broadcasted_iota(jnp.int32, (total_rows, ep_count), 0)
    slot_experts = lax.broadcasted_iota(jnp.int32, (total_rows, ep_count), 1)
    spread = jnp.where(slot_rows // cap == slot_experts, 1.0, 0.0).astype(bf16)
    slot_of_row = lax.broadcasted_iota(jnp.int32, (total_rows, seq_count), 0) % cap
    hits = jnp.dot(spread, slots, preferred_element_type=f32) == slot_of_row.astype(f32)
    chooser = jnp.where(hits, 1.0, 0.0)
    placement = chooser.astype(bf16)

    loads[0].wait()
    for index in range(2):
        columns = slice(index * half, (index + 1) * half)
        part_buf[index] = jnp.dot(
            mixed_ref[...], w_out_ref[:, columns], preferred_element_type=f32
        )
    pl.semaphore_wait(barrier, ep_count)

    def pair_copy(source, target, send_sem, recv_sem):
        return pltpu.make_async_remote_copy(
            src_ref=source,
            dst_ref=target,
            send_sem=send_sem,
            recv_sem=recv_sem,
            device_id=(me, other),
            device_id_type=mesh_ids,
        )

    part_copy = pair_copy(part_buf, part_recv, part_sems.at[0], part_sems.at[1])
    part_copy.start()
    part_copy.wait()

    squares = jnp.zeros((seq_count, 1), f32)
    for index in range(2):
        columns = slice(index * half, (index + 1) * half)
        mixer_out = (part_buf[index] + part_recv[index]).astype(bf16)
        mid = (tokens_ref[:, columns].astype(f32) + mixer_out.astype(f32)).astype(bf16)
        mid_buf[index] = mid
        mid32 = mid.astype(f32)
        squares = squares + jnp.sum(mid32 * mid32, axis=1, keepdims=True)
    factor = lax.rsqrt(squares / width + 1e-06)
    for index in range(2):
        columns = slice(index * half, (index + 1) * half)
        norm_buf[index] = (
            mid_buf[index].astype(f32) * factor * norm_ref[columns].reshape(1, half).astype(f32)
        ).astype(bf16)

    own_norm = norm_buf[core]
    for index in range(n_blocks):
        rows = jnp.dot(
            placement[index * block_rows : (index + 1) * block_rows, :],
            own_norm,
            preferred_element_type=f32,
        ).astype(bf16)
        send_buf[index * per_block : (index + 1) * per_block] = rows.reshape(per_block, cap, half)

    def out_copy(step):
        peer = peer_at(step)
        return pltpu.make_async_remote_copy(
            src_ref=send_buf.at[peer],
            dst_ref=rows_buf.at[core, me],
            send_sem=out_send_sems.at[step],
            recv_sem=out_recv_sems.at[step],
            device_id=(peer, core),
            device_id_type=mesh_ids,
        )

    def rows_copy(step):
        source = lax.rem(me + ep_count - step, ep_count)
        return pair_copy(
            rows_buf.at[core, source],
            rows_buf.at[core, source],
            pair_send_sems.at[step],
            pair_recv_sems.at[step],
        )

    def rows_arrival(step):
        source = lax.rem(me + ep_count - step, ep_count)
        return pair_copy(
            rows_buf.at[other, source],
            rows_buf.at[other, source],
            pair_send_sems.at[step],
            pair_recv_sems.at[step],
        )

    def start_out(index, carry):
        out_copy(step_at(index)).start()
        return carry

    lax.fori_loop(0, ep_count - 1, start_out, 0)
    rows_buf[core, me] = send_buf[me]
    rows_copy(0).start()

    rows_dims = (((1,), (1,)), ((), ()))
    group_logit = jnp.zeros(group_hit.shape, f32)
    expert_logit = jnp.zeros(uses.shape, f32)
    for index in range(2):
        columns = slice(index * half, (index + 1) * half)
        group_logit += lax.dot_general(
            router_group_ref[:, columns], norm_buf[index], rows_dims, preferred_element_type=f32
        )
        expert_logit += lax.dot_general(
            router_expert_ref[:, columns], norm_buf[index], rows_dims, preferred_element_type=f32
        )
    group_prob = jax.nn.sigmoid(jnp.sum(group_logit * group_hit, axis=0, keepdims=True))
    scores = jax.nn.sigmoid(expert_logit) * uses
    weights = group_prob * scores / jnp.sum(scores, axis=0, keepdims=True)
    weights_high = weights.astype(bf16)
    weights_low = (weights - weights_high.astype(f32)).astype(bf16)
    combine_high = (jnp.dot(spread, weights_high, preferred_element_type=f32) * chooser).T
    combine_low = (jnp.dot(spread, weights_low, preferred_element_type=f32) * chooser).T
    combine_high = combine_high.astype(bf16)
    combine_low = combine_low.astype(bf16)
    mid_ref[...] = mid_buf[core]

    def relay(index, carry):
        step = step_at(ep_count - 2 - index)
        out_copy(step).wait_recv()
        rows_copy(step).start()
        return carry

    lax.fori_loop(0, ep_count - 1, relay, 0)

    def arrive(step, carry):
        rows_arrival(step).wait_recv()
        return carry

    lax.fori_loop(0, ep_count, arrive, 0)

    for load in loads[1:]:
        load.wait()
    for index in range(n_blocks):
        experts = slice(index * per_block, (index + 1) * per_block)
        gate_part = jnp.zeros((block_rows, gate_ref.shape[1]), f32)
        up_part = jnp.zeros((block_rows, gate_ref.shape[1]), f32)
        for piece in range(2):
            columns = slice(piece * half, (piece + 1) * half)
            rows = rows_buf[piece, experts].reshape(block_rows, half)
            gate_part += jnp.dot(rows, gate_ref[columns, :], preferred_element_type=f32)
            up_part += jnp.dot(rows, up_ref[columns, :], preferred_element_type=f32)
        hidden = (gate_part / (1.0 + jnp.exp(-gate_part)) * up_part).astype(bf16)
        hidden_buf[experts] = hidden.reshape(per_block, cap, gate_ref.shape[1])

    n_parts = term_send.shape[0]
    per_part = ep_count // n_parts
    first_part = me // per_part

    def part_at(index):
        return lax.rem(first_part + index + n_parts // 2, n_parts)

    def term_copy(part):
        return pair_copy(
            term_send.at[part],
            term_recv.at[part],
            term_send_sems.at[part],
            term_recv_sems.at[part],
        )

    def part_term(part, which):
        hidden = hidden_buf[pl.ds(part * per_part, per_part)]
        hidden = hidden.reshape(per_part * cap, gate_ref.shape[1])
        term = jnp.dot(hidden, down_ref[which], preferred_element_type=f32)
        return term.astype(bf16).reshape(per_part, cap, half)

    def back_copy(peer):
        return pltpu.make_async_remote_copy(
            src_ref=result_buf.at[peer],
            dst_ref=back_buf.at[me],
            send_sem=back_send_sems.at[peer],
            recv_sem=back_recv_sems.at[me],
            device_id=(peer, core),
            device_id_type=mesh_ids,
        )

    def back_arrival(peer):
        return pltpu.make_async_remote_copy(
            src_ref=result_buf.at[peer],
            dst_ref=back_buf.at[peer],
            send_sem=back_send_sems.at[peer],
            recv_sem=back_recv_sems.at[peer],
            device_id=(peer, core),
            device_id_type=mesh_ids,
        )

    def send_terms(index, carry):
        part = part_at(index)
        term_send[part] = part_term(part, other)
        term_copy(part).start()
        return carry

    lax.fori_loop(0, n_parts, send_terms, 0)

    def own_terms(index, carry):
        part = part_at(index)
        term_own[part] = part_term(part, core)
        return carry

    lax.fori_loop(0, n_parts, own_terms, 0)

    def finish_part(index, carry):
        part = part_at(index)
        term_copy(part).wait_recv()
        total = term_own[part].astype(f32) + term_recv[part].astype(f32)
        result_buf[pl.ds(part * per_part, per_part)] = total.astype(bf16)

        def start_back(inner, carry_inner):
            peer = part * per_part + inner

            @pl.when(peer != me)
            def _():
                back_copy(peer).start()

            return carry_inner

        lax.fori_loop(0, per_part, start_back, 0)
        return carry

    lax.fori_loop(0, n_parts, finish_part, 0)
    back_buf[me] = result_buf[me]

    def finish_sends(step, carry):
        out_copy(step).wait_send()
        back_arrival(peer_at(step)).wait_recv()
        back_copy(peer_at(step)).wait_send()
        return carry

    lax.fori_loop(1, ep_count, finish_sends, 0)

    def finish_pair(step, carry):
        rows_copy(step).wait_send()
        return carry

    lax.fori_loop(0, ep_count, finish_pair, 0)

    def finish_terms(part, carry):
        term_copy(part).wait_send()
        return carry

    lax.fori_loop(0, n_parts, finish_terms, 0)

    back = back_buf[...].reshape(total_rows, half)
    moe_out = jnp.dot(combine_high, back, preferred_element_type=f32)
    moe_out += jnp.dot(combine_low, back, preferred_element_type=f32)
    moe_ref[...] = moe_out


def shards(
    tokens_in,
    state_in,
    norm_mix,
    w_recept,
    w_key,
    w_value,
    decay_down,
    decay_up,
    decay_base,
    iclr_down,
    iclr_up,
    iclr_base,
    key_scale,
    key_mix,
    w_out,
    norm_moe,
    router_group,
    router_expert,
    routes,
    expert_gate,
    expert_up,
    expert_down,
):
    f32 = jnp.float32
    bf16 = jnp.bfloat16
    seq_count, width_model = tokens_in.shape
    heads_here, head_size = state_in.shape[1], state_in.shape[3]
    channels = heads_here * head_size
    tp_count = lax.axis_size("tp")
    ep_count = lax.axis_size("ep")
    dma = pltpu.SemaphoreType.DMA
    vmem = pl.BlockSpec(memory_space=pltpu.VMEM)
    anywhere = pl.BlockSpec(memory_space=pl.ANY)
    n_chunks = 4 if seq_count % 4 == 0 else 1
    mixed, state_out = pl.pallas_call(
        mixer_kernel,
        out_shape=(
            jax.ShapeDtypeStruct((seq_count, channels), bf16),
            jax.ShapeDtypeStruct(state_in.shape, f32),
        ),
        in_specs=[vmem] * 2 + [anywhere] * 3 + [vmem] * 8 + [anywhere],
        out_specs=(vmem, anywhere),
        scratch_shapes=[
            pltpu.VMEM((3, width_model, channels), bf16),
            pltpu.VMEM(state_in.shape, f32),
            pltpu.VMEM(state_in.shape, f32),
            pltpu.VMEM((5, heads_here, seq_count, head_size), f32),
            pltpu.VMEM((channels, seq_count), f32),
            pltpu.VMEM((channels, seq_count), f32),
            dma((3,)),
            dma((n_chunks,)),
            dma((n_chunks,)),
        ],
        compiler_params=pltpu.CompilerParams(vmem_limit_bytes=60 * 1024 * 1024),
    )(
        tokens_in,
        norm_mix,
        w_recept,
        w_key,
        w_value,
        decay_down.T,
        decay_up,
        decay_base,
        iclr_down.T,
        iclr_up,
        iclr_base,
        key_scale,
        key_mix,
        state_in,
    )
    top_count = routes.shape[1]
    half_width = width_model // tp_count
    limit = max(2, 2 * seq_count * top_count // ep_count)
    cap = -(-limit // 16) * 16
    block_rows = min(ep_count * cap, 256)
    n_parts = min(4, ep_count)
    per_part = ep_count // n_parts
    hidden_width = expert_gate.shape[2]
    moe_out, mid_half = pl.pallas_call(
        functools.partial(moe_kernel, ep_count, block_rows),
        out_shape=(
            jax.ShapeDtypeStruct((seq_count, half_width), f32),
            jax.ShapeDtypeStruct((seq_count, half_width), bf16),
        ),
        in_specs=[vmem, anywhere] + [vmem] * 5 + [anywhere] * 3,
        out_specs=(vmem, vmem),
        scratch_shapes=[
            pltpu.VMEM((width_model, hidden_width), bf16),
            pltpu.VMEM((width_model, hidden_width), bf16),
            pltpu.VMEM((tp_count, hidden_width, half_width), bf16),
            pltpu.VMEM(w_out.shape, bf16),
            pltpu.VMEM((tp_count, seq_count, half_width), f32),
            pltpu.VMEM((tp_count, seq_count, half_width), f32),
            pltpu.VMEM((tp_count, seq_count, half_width), bf16),
            pltpu.VMEM((tp_count, seq_count, half_width), bf16),
            pltpu.VMEM((ep_count, cap, half_width), bf16),
            pltpu.VMEM((tp_count, ep_count, cap, half_width), bf16),
            pltpu.VMEM((ep_count, cap, hidden_width), bf16),
            pltpu.VMEM((n_parts, per_part, cap, half_width), bf16),
            pltpu.VMEM((n_parts, per_part, cap, half_width), bf16),
            pltpu.VMEM((n_parts, per_part, cap, half_width), bf16),
            pltpu.VMEM((ep_count, cap, half_width), bf16),
            pltpu.VMEM((ep_count, cap, half_width), bf16),
            dma((2,)),
            dma((ep_count,)),
            dma((ep_count,)),
            dma((ep_count,)),
            dma((ep_count,)),
            dma((n_parts,)),
            dma((n_parts,)),
            dma((ep_count,)),
            dma((ep_count,)),
            dma((5,)),
        ],
        compiler_params=pltpu.CompilerParams(
            collective_id=0, has_side_effects=True, vmem_limit_bytes=60 * 1024 * 1024
        ),
    )(
        mixed,
        w_out,
        tokens_in,
        norm_moe,
        router_group.T,
        router_expert.T,
        routes.T,
        expert_gate,
        expert_up,
        expert_down,
    )
    layer_out = (mid_half.astype(f32) + moe_out).astype(bf16)
    return (layer_out, state_out)


def solution(mesh):
    in_specs = (
        P("ep", None),
        P("ep", "tp", None, None),
        P(),
        P(None, "tp"),
        P(None, "tp"),
        P(None, "tp"),
        P(),
        P(None, "tp"),
        P("tp"),
        P(),
        P(None, "tp"),
        P("tp"),
        P("tp"),
        P("tp"),
        P("tp", None),
        P(),
        P(),
        P(),
        P("ep", None),
        P("ep", None, "tp"),
        P("ep", None, "tp"),
        P("ep", "tp", None),
    )
    out_specs = (P("ep", "tp"), P("ep", "tp", None, None))
    return jax.shard_map(shards, mesh=mesh, in_specs=in_specs, out_specs=out_specs, check_vma=False)
```

profile of v0, /device:TPU:0, one launch (start us, length us, event | category | flops | bytes accessed | tf_op | source)
XLA Modules:
  0.0 56.0 jit_solution(8745259136601089880)
XLA Ops:
  0.6 14.2 %shard_map.221 = (bf16[32,256]{1,0:T(8,128)(2,1)}, f32[32,4,64,64]{3,2,1,0:T(8,128)}) custom-call(bf16[32,2048]{1,0:T(8,128)(2,1)} %tokens_ref.3, bf16[2048]{0:T(1024)(128)(2,1)} %norm_ref.2, bf16[2048,256]{1,0:T(8,128)(2,1)} %w_recept_hbm.1, bf16[2048,256]{1,0:T(8,128)(2,1)} %w_key_hbm.1, bf16[2048,256]{1,0:T(8,128)(2,1)} %w_value_hbm.1, ...), custom_call_target="tpu_custom_call" | custom-call | tf_op jit(solution)/shard_map/pallas_call | solution.py:505
  14.9 39.5 %shard_map.222 = (f32[32,1024]{1,0:T(8,128)}, bf16[32,1024]{1,0:T(8,128)(2,1)}) custom-call(bf16[32,256]{1,0:T(8,128)(2,1)} %get-tuple-element.6.mixed_ref, bf16[256,2048]{1,0:T(8,128)(2,1)} %w_out_hbm.1, bf16[32,2048]{1,0:T(8,128)(2,1)} %tokens_ref.3, bf16[2048]{0:T(1024)(128)(2,1)} %norm_ref.3, bf16[2,2048]{1,0:T(2,128)(2,1)} %bitcast.8, ...), custom_call_target="tpu_custom_call" | custom-call | tf_op jit(solution)/shard_map/pallas_call | solution.py:549
  54.4 1.6 %add_convert_fusion = bf16[32,1024]{1,0:T(8,128)(2,1)} fusion(f32[32,1024]{1,0:T(8,128)} %get-tuple-element.8, bf16[32,1024]{1,0:T(8,128)(2,1)} %get-tuple-element.7), kind=kLoop, calls=%fused_computation | loop fusion | flops 98304 | bytes 262144 | tf_op jit(solution)/shard_map/convert_element_type | solution.py:600
where the time goes:
time: 56.2 us; the launch traced here: 56 us
  Pallas kernels  53.8 us (96%)
  other arithmetic  1.55 us (3%)
  between operations  0.65 us (1%)
    pallas_call x1, Pallas kernels, shards(): pl.pallas_call(functools.partial(moe_kernel, ep_count, block_rows), out_s...  39.5 us
    pallas_call x1, Pallas kernels, shards(): pl.pallas_call(mixer_kernel, out_shape=(jax.ShapeDtypeStruct((seq_count,...  14.2 us
    convert_element_type x1, other arithmetic, shards(): layer_out = (mid_half.astype(f32) + moe_out).astype(bf16)  1.55 us

commit v1 on v0

--- a/solution.py
+++ b/solution.py
@@ -9,31 +9,10 @@
 
 
 def mixer_kernel(
-    tokens_ref,
-    norm_ref,
-    w_recept_hbm,
-    w_key_hbm,
-    w_value_hbm,
-    decay_down_ref,
-    decay_up_ref,
-    decay_base_ref,
-    iclr_down_ref,
-    iclr_up_ref,
-    iclr_base_ref,
-    key_scale_ref,
-    key_mix_ref,
-    state_hbm,
-    mixed_ref,
-    state_out_hbm,
-    weights,
-    state_buf,
-    out_buf,
-    vectors,
-    value_t,
-    mixed_t,
-    weight_sems,
-    in_sems,
-    out_sems,
+    tokens_ref, norm_ref, w_recept_hbm, w_key_hbm, w_value_hbm, decay_down_ref, decay_up_ref, decay_base_ref,
+    iclr_down_ref, iclr_up_ref, iclr_base_ref, key_scale_ref, key_mix_ref, state_hbm,
+    mixed_ref, state_out_hbm,
+    weights, state_buf, out_buf, weight_sems, in_sems, out_sems,
 ):
     f32 = jnp.float32
     bf16 = jnp.bfloat16
@@ -45,7 +24,7 @@
     rows_dims = (((1,), (1,)), ((), ()))
     weight_loads = [
         pltpu.make_async_copy(source, weights.at[index], weight_sems.at[index])
-        for index, source in enumerate((w_key_hbm, w_value_hbm, w_recept_hbm))
+        for index, source in enumerate((w_key_hbm, w_recept_hbm, w_value_hbm))
     ]
     for load in weight_loads:
         load.start()
@@ -78,51 +57,58 @@
         iclr_base_ref[...].reshape(1, channels)
         + jnp.dot(iclr_low, iclr_up_ref[...], preferred_element_type=f32)
     )
-    projected = []
-    for index in range(3):
+
+    def project(index):
         weight_loads[index].wait()
         rows = jnp.dot(normed, weights[index], preferred_element_type=f32)
-        projected.append(rows.astype(bf16).astype(f32))
-    key, value, recept = projected
-    value_t[...] = value.T
+        return rows.astype(bf16).astype(f32)
+
+    key = project(0)
     scaled = key * key_scale_ref[...].reshape(1, channels).astype(f32)
     key_mod = key * (1.0 + (rate - 1.0) * key_mix_ref[...].reshape(1, channels).astype(f32))
-    for head in range(heads):
-        span = slice(head * head_size, (head + 1) * head_size)
+    spans = [slice(head * head_size, (head + 1) * head_size) for head in range(heads)]
+    units = []
+    for span in spans:
         part = scaled[:, span]
-        unit = part * lax.rsqrt(jnp.sum(part * part, axis=1, keepdims=True) + 1e-06)
-        vectors[0, head] = decays[:, span]
-        vectors[1, head] = unit
-        vectors[2, head] = unit * rate[:, span]
-        vectors[3, head] = key_mod[:, span]
-        vectors[4, head] = recept[:, span]
-
-    lanes = lax.broadcasted_iota(jnp.int32, (head_size, seq_count), 1)
-
-    def update(seq, carry):
-        here = lanes == seq
-        for head in range(heads):
-            span = slice(head * head_size, (head + 1) * head_size)
-            row = pl.ds(seq, 1)
-            state = state_buf[seq, head]
-            removed = jnp.sum(state * vectors[1, head, row, :], axis=1, keepdims=True)
-            column = jnp.sum(jnp.where(here, value_t[span, :], 0.0), axis=1, keepdims=True)
-            state = (
-                state * vectors[0, head, row, :]
-                - removed * vectors[2, head, row, :]
-                + column * vectors[3, head, row, :]
+        units.append(part * lax.rsqrt(jnp.sum(part * part, axis=1, keepdims=True) + 1e-06))
+    recept = project(1)
+    readers, writers, gains = [], [], []
+    for head, span in enumerate(spans):
+        unit, query = units[head], recept[:, span]
+        drop = unit * rate[:, span]
+        shift = jnp.sum(drop * query, axis=1, keepdims=True)
+        gains.append(jnp.sum(key_mod[:, span] * query, axis=1, keepdims=True))
+        reader = decays[:, span] * query - unit * shift
+        readers.append(jnp.concatenate([unit, reader], axis=0).astype(bf16))
+        writers.append(jnp.concatenate([-drop, key_mod[:, span]], axis=0).astype(bf16))
+    value = project(2)
+    value_t = jnp.concatenate([value, value], axis=0).T
+
+    lanes = lax.broadcasted_iota(jnp.int32, (per_chunk, head_size, 2 * seq_count), 2)
+    seqs = lax.broadcasted_iota(jnp.int32, (per_chunk, head_size, 2 * seq_count), 0)
+    first = lanes < seq_count
+    owner = jnp.where(first, lanes, lanes - seq_count)
+    totals = [jnp.zeros((head_size, 2 * seq_count), f32) for _ in range(heads)]
+    for index in range(n_chunks):
+        rows = slice(index * per_chunk, (index + 1) * per_chunk)
+        here = owner == seqs + index * per_chunk
+        state_loads[index].wait()
+        for head, span in enumerate(spans):
+            state = state_buf[rows, head]
+            flat = state.reshape(per_chunk * head_size, head_size).astype(bf16)
+            read = lax.dot_general(flat, readers[head], rows_dims, preferred_element_type=f32)
+            read = read.reshape(per_chunk, head_size, 2 * seq_count)
+            totals[head] += jnp.sum(jnp.where(here, read, 0.0), axis=0)
+            terms = jnp.where(here, jnp.where(first, read, value_t[span, :][None]), 0.0)
+            terms = terms.reshape(per_chunk * head_size, 2 * seq_count).astype(bf16)
+            change = jnp.dot(terms, writers[head], preferred_element_type=f32)
+            out_buf[rows, head] = state * decays[rows, span][:, None, :] + change.reshape(
+                per_chunk, head_size, head_size
             )
-            out_buf[seq, head] = state
-            mixed = jnp.sum(state * vectors[4, head, row, :], axis=1, keepdims=True)
-            mixed_t[span, :] = jnp.where(here, mixed, mixed_t[span, :])
-        return carry
-
-    mixed_t[...] = jnp.zeros_like(mixed_t)
-    for index in range(n_chunks):
-        state_loads[index].wait()
-        lax.fori_loop(index * per_chunk, (index + 1) * per_chunk, update, 0, unroll=2)
         state_stores[index].start()
-    mixed_ref[...] = mixed_t[...].T.astype(bf16)
+    total = jnp.concatenate(totals, axis=0).T[seq_count:]
+    for head, span in enumerate(spans):
+        mixed_ref[:, span] = (total[:, span] + value[:, span] * gains[head]).astype(bf16)
     for store in state_stores:
         store.wait()
 
@@ -501,7 +487,7 @@
     dma = pltpu.SemaphoreType.DMA
     vmem = pl.BlockSpec(memory_space=pltpu.VMEM)
     anywhere = pl.BlockSpec(memory_space=pl.ANY)
-    n_chunks = 4 if seq_count % 4 == 0 else 1
+    n_chunks = 2 if seq_count % 2 == 0 else 1
     mixed, state_out = pl.pallas_call(
         mixer_kernel,
         out_shape=(
@@ -514,9 +500,6 @@
             pltpu.VMEM((3, width_model, channels), bf16),
             pltpu.VMEM(state_in.shape, f32),
             pltpu.VMEM(state_in.shape, f32),
-            pltpu.VMEM((5, heads_here, seq_count, head_size), f32),
-            pltpu.VMEM((channels, seq_count), f32),
-            pltpu.VMEM((channels, seq_count), f32),
             dma((3,)),
             dma((n_chunks,)),
             dma((n_chunks,)),

time: 56.2 us -> 49.7 us (0.88)
  Pallas kernels: 53.8 us -> 47.3 us
    pallas_call x1, Pallas kernels: 14.2 us -> 7.78 us  [shards(): pl.pallas_call(mixer_kernel, out_shape=(jax.ShapeDtypeStruct((seq_count,...]
where the time goes in v1:
time: 49.7 us; the launch traced here: 49.5 us
  Pallas kernels  47.3 us (95%)
  other arithmetic  1.55 us (3%)
  between operations  0.65 us (1%)
    pallas_call x1, Pallas kernels, shards(): pl.pallas_call(functools.partial(moe_kernel, ep_count, block_rows), out_s...  39.5 us
    pallas_call x1, Pallas kernels, shards(): pl.pallas_call(mixer_kernel, out_shape=(jax.ShapeDtypeStruct((seq_count,...  7.78 us
    convert_element_type x1, other arithmetic, shards(): layer_out = (mid_half.astype(f32) + moe_out).astype(bf16)  1.55 us

profile of v1, /device:TPU:0, one launch (start us, length us, event | category | flops | bytes accessed | tf_op | source)
XLA Modules:
  0.0 49.5 jit_solution(11679130801460571291)
XLA Ops:
  0.6 7.8 %shard_map.221 = (bf16[32,256]{1,0:T(8,128)(2,1)}, f32[32,4,64,64]{3,2,1,0:T(8,128)}) custom-call(bf16[32,2048]{1,0:T(8,128)(2,1)} %tokens_ref.3, bf16[2048]{0:T(1024)(128)(2,1)} %norm_ref.2, bf16[2048,256]{1,0:T(8,128)(2,1)} %w_recept_hbm.1, bf16[2048,256]{1,0:T(8,128)(2,1)} %w_key_hbm.1, bf16[2048,256]{1,0:T(8,128)(2,1)} %w_value_hbm.1, ...), custom_call_target="tpu_custom_call" | custom-call | tf_op jit(solution)/shard_map/pallas_call | solution.py:491
  8.4 39.5 %shard_map.222 = (f32[32,1024]{1,0:T(8,128)}, bf16[32,1024]{1,0:T(8,128)(2,1)}) custom-call(bf16[32,256]{1,0:T(8,128)(2,1)} %get-tuple-element.6.mixed_ref, bf16[256,2048]{1,0:T(8,128)(2,1)} %w_out_hbm.1, bf16[32,2048]{1,0:T(8,128)(2,1)} %tokens_ref.3, bf16[2048]{0:T(1024)(128)(2,1)} %norm_ref.3, bf16[2,2048]{1,0:T(2,128)(2,1)} %bitcast.8, ...), custom_call_target="tpu_custom_call" | custom-call | tf_op jit(solution)/shard_map/pallas_call | solution.py:532
  48.0 1.6 %add_convert_fusion = bf16[32,1024]{1,0:T(8,128)(2,1)} fusion(f32[32,1024]{1,0:T(8,128)} %get-tuple-element.8, bf16[32,1024]{1,0:T(8,128)(2,1)} %get-tuple-element.7), kind=kLoop, calls=%fused_computation | loop fusion | flops 98304 | bytes 262144 | tf_op jit(solution)/shard_map/convert_element_type | solution.py:583

commit v2 on v1

--- a/solution.py
+++ b/solution.py
@@ -115,7 +115,6 @@
 
 def moe_kernel(
     ep_count,
-    block_rows,
     mixed_ref,
     w_out_hbm,
     tokens_ref,
@@ -126,8 +125,7 @@
     gate_hbm,
     up_hbm,
     down_hbm,
-    moe_ref,
-    mid_ref,
+    out_ref,
     gate_ref,
     up_ref,
     down_ref,
@@ -136,23 +134,37 @@
     part_recv,
     mid_buf,
     norm_buf,
+    place_own,
+    place_all,
+    comb_own,
+    comb_all,
+    rows_own,
+    rows_all,
     send_buf,
     rows_buf,
-    hidden_buf,
     term_send,
-    term_own,
     term_recv,
     result_buf,
     back_buf,
+    sum_send,
+    sum_recv,
     part_sems,
-    out_send_sems,
-    out_recv_sems,
+    place_send_sems,
+    place_recv_sems,
+    comb_send_sems,
+    comb_recv_sems,
+    cross_send_sems,
+    cross_recv_sems,
+    fan_send_sems,
+    fan_recv_sems,
     pair_send_sems,
     pair_recv_sems,
     term_send_sems,
     term_recv_sems,
     back_send_sems,
     back_recv_sems,
+    sum_send_sems,
+    sum_recv_sems,
     load_sems,
 ):
     f32 = jnp.float32
@@ -162,28 +174,63 @@
     other = 1 - core
     seq_count, width = tokens_ref.shape
     half = width // 2
-    cap = send_buf.shape[1]
+    cap = send_buf.shape[2]
     total_rows = ep_count * cap
-    per_block = block_rows // cap
-    n_blocks = total_rows // block_rows
     mesh_ids = pl.DeviceIdType.MESH
-
-    def peer_at(step):
-        return lax.rem(me + step, ep_count)
-
-    def step_at(index):
-        return 1 + lax.rem(index + ep_count // 2 - 1, ep_count - 1)
+    n_groups = router_group_ref.shape[0]
+    size = ep_count // n_groups
+    group = me // size
+    rank = me % size
+    block_rows = size * cap
+    hidden_width = gate_ref.shape[1]
+    power = size & (size - 1) == 0
+    steps = sorted(range(1, size), key=lambda step: -bin(step).count("1"))
+
+    def flip(step):
+        moved = rank * 0
+        bit = 1
+        while bit < size:
+            value = rank // bit % 2
+            moved = moved + bit * ((1 - value) if step & bit else value)
+            bit *= 2
+        return moved
+
+    to_rank = {s: flip(s) if power else (rank + s) % size for s in steps}
+    from_rank = {s: flip(s) if power else (rank + size - s) % size for s in steps}
+    base = group * size
+
+    def each(low, high, visit):
+        if high - low <= 2:
+            for index in range(low, high):
+                visit(index)
+        else:
+            lax.fori_loop(low, high, lambda index, carry: (visit(index), carry)[1], 0)
+
+    def source_group(block):
+        return (group + n_groups - block) % n_groups
+
+    def target_group(block):
+        return (group + block) % n_groups
+
+    def remote(source, target, send_sem, recv_sem, device):
+        return pltpu.make_async_remote_copy(
+            src_ref=source,
+            dst_ref=target,
+            send_sem=send_sem,
+            recv_sem=recv_sem,
+            device_id=device,
+            device_id_type=mesh_ids,
+        )
 
     barrier = pltpu.get_barrier_semaphore()
-    pl.semaphore_signal(barrier, inc=1, device_id=(me, other), device_id_type=mesh_ids)
-
-    def greet(step, carry):
-        pl.semaphore_signal(
-            barrier, inc=1, device_id=(peer_at(step), core), device_id_type=mesh_ids
-        )
-        return carry
-
-    lax.fori_loop(1, ep_count, greet, 0)
+
+    def greet(device):
+        pl.semaphore_signal(barrier, inc=1, device_id=device, device_id_type=mesh_ids)
+
+    each(1, n_groups, lambda block: greet((target_group(block) * size + rank, core)))
+    for step in steps:
+        greet((base + to_rank[step], core))
+    greet((me, other))
 
     loads = [
         pltpu.make_async_copy(w_out_hbm, w_out_ref, load_sems.at[0]),
@@ -195,15 +242,12 @@
     for load in loads:
         load.start()
 
-    n_groups = router_group_ref.shape[0]
     expert_ids = lax.broadcasted_iota(jnp.int32, (ep_count, seq_count), 0)
     uses = jnp.zeros((ep_count, seq_count), f32)
     for index in range(routes_ref.shape[0]):
         uses += jnp.where(routes_ref[index : index + 1, :] == expert_ids, 1.0, 0.0)
     group_ids = lax.broadcasted_iota(jnp.int32, (n_groups, seq_count), 0)
-    group_hit = jnp.where(
-        routes_ref[0:1, :] // (ep_count // n_groups) == group_ids, 1.0, 0.0
-    )
+    group_hit = jnp.where(routes_ref[0:1, :] // size == group_ids, 1.0, 0.0)
     row_ids = lax.broadcasted_iota(jnp.int32, (seq_count, seq_count), 0)
     column_ids = lax.broadcasted_iota(jnp.int32, (seq_count, seq_count), 1)
     earlier = jnp.where(row_ids < column_ids, 1.0, 0.0).astype(bf16)
@@ -215,7 +259,8 @@
     slot_of_row = lax.broadcasted_iota(jnp.int32, (total_rows, seq_count), 0) % cap
     hits = jnp.dot(spread, slots, preferred_element_type=f32) == slot_of_row.astype(f32)
     chooser = jnp.where(hits, 1.0, 0.0)
-    placement = chooser.astype(bf16)
+    place_own[...] = chooser.astype(bf16).reshape(n_groups, block_rows, seq_count)
+    place_all[group] = place_own[group]
 
     loads[0].wait()
     for index in range(2):
@@ -223,20 +268,35 @@
         part_buf[index] = jnp.dot(
             mixed_ref[...], w_out_ref[:, columns], preferred_element_type=f32
         )
-    pl.semaphore_wait(barrier, ep_count)
-
-    def pair_copy(source, target, send_sem, recv_sem):
-        return pltpu.make_async_remote_copy(
-            src_ref=source,
-            dst_ref=target,
-            send_sem=send_sem,
-            recv_sem=recv_sem,
-            device_id=(me, other),
-            device_id_type=mesh_ids,
-        )
-
-    part_copy = pair_copy(part_buf, part_recv, part_sems.at[0], part_sems.at[1])
+    pl.semaphore_wait(barrier, (n_groups - 1) + (size - 1) + 1)
+
+    part_copy = remote(part_buf, part_recv, part_sems.at[0], part_sems.at[1], (me, other))
     part_copy.start()
+
+    def across(block, buffer, target, send_sems, recv_sems):
+        goal = target_group(block)
+        return remote(
+            buffer.at[goal] if buffer is not rows_own else buffer,
+            target.at[group],
+            send_sems.at[block],
+            recv_sems.at[group],
+            (goal * size + rank, core),
+        )
+
+    def across_arrival(block, buffer, target, send_sems, recv_sems):
+        origin = source_group(block)
+        return remote(
+            buffer.at[origin] if buffer is not rows_own else buffer,
+            target.at[origin],
+            send_sems.at[block],
+            recv_sems.at[origin],
+            (origin * size + rank, core),
+        )
+
+    place_args = (place_own, place_all, place_send_sems, place_recv_sems)
+    comb_args = (comb_own, comb_all, comb_send_sems, comb_recv_sems)
+    cross_args = (rows_own, rows_all, cross_send_sems, cross_recv_sems)
+    each(1, n_groups, lambda block: across(block, *place_args).start())
     part_copy.wait()
 
     squares = jnp.zeros((seq_count, 1), f32)
@@ -254,51 +314,58 @@
             mid_buf[index].astype(f32) * factor * norm_ref[columns].reshape(1, half).astype(f32)
         ).astype(bf16)
 
-    own_norm = norm_buf[core]
-    for index in range(n_blocks):
-        rows = jnp.dot(
-            placement[index * block_rows : (index + 1) * block_rows, :],
-            own_norm,
-            preferred_element_type=f32,
-        ).astype(bf16)
-        send_buf[index * per_block : (index + 1) * per_block] = rows.reshape(per_block, cap, half)
-
-    def out_copy(step):
-        peer = peer_at(step)
-        return pltpu.make_async_remote_copy(
-            src_ref=send_buf.at[peer],
-            dst_ref=rows_buf.at[core, me],
-            send_sem=out_send_sems.at[step],
-            recv_sem=out_recv_sems.at[step],
-            device_id=(peer, core),
-            device_id_type=mesh_ids,
-        )
-
-    def rows_copy(step):
-        source = lax.rem(me + ep_count - step, ep_count)
-        return pair_copy(
+    rows_own[...] = norm_buf[core]
+    each(1, n_groups, lambda block: across(block, *cross_args).start())
+    rows_all[group] = rows_own[...]
+
+    def fan_copy(block, step):
+        source = source_group(block) * size + rank
+        return remote(
+            send_buf.at[block, to_rank[step]],
+            rows_buf.at[core, source],
+            fan_send_sems.at[block, step],
+            fan_recv_sems.at[source],
+            (base + to_rank[step], core),
+        )
+
+    def fan_arrival(block, step):
+        source = source_group(block) * size + from_rank[step]
+        return remote(
+            send_buf.at[block, to_rank[step]],
+            rows_buf.at[core, source],
+            fan_send_sems.at[block, step],
+            fan_recv_sems.at[source],
+            (base + from_rank[step], core),
+        )
+
+    def rows_copy(source):
+        return remote(
             rows_buf.at[core, source],
             rows_buf.at[core, source],
-            pair_send_sems.at[step],
-            pair_recv_sems.at[step],
-        )
-
-    def rows_arrival(step):
-        source = lax.rem(me + ep_count - step, ep_count)
-        return pair_copy(
+            pair_send_sems.at[source],
+            pair_recv_sems.at[source],
+            (me, other),
+        )
+
+    def rows_arrival(source):
+        return remote(
             rows_buf.at[other, source],
             rows_buf.at[other, source],
-            pair_send_sems.at[step],
-            pair_recv_sems.at[step],
-        )
-
-    def start_out(index, carry):
-        out_copy(step_at(index)).start()
-        return carry
-
-    lax.fori_loop(0, ep_count - 1, start_out, 0)
-    rows_buf[core, me] = send_buf[me]
-    rows_copy(0).start()
+            pair_send_sems.at[source],
+            pair_recv_sems.at[source],
+            (me, other),
+        )
+
+    def fan_out(block):
+        origin = source_group(block)
+        rows = jnp.dot(place_all[origin], rows_all[origin], preferred_element_type=f32)
+        send_buf[block] = rows.astype(bf16).reshape(size, cap, half)
+        for step in steps:
+            fan_copy(block, step).start()
+        rows_buf[core, origin * size + rank] = send_buf[block, rank]
+        rows_copy(origin * size + rank).start()
+
+    fan_out(0)
 
     rows_dims = (((1,), (1,)), ((), ()))
     group_logit = jnp.zeros(group_hit.shape, f32)
@@ -314,143 +381,132 @@
     group_prob = jax.nn.sigmoid(jnp.sum(group_logit * group_hit, axis=0, keepdims=True))
     scores = jax.nn.sigmoid(expert_logit) * uses
     weights = group_prob * scores / jnp.sum(scores, axis=0, keepdims=True)
-    weights_high = weights.astype(bf16)
-    weights_low = (weights - weights_high.astype(f32)).astype(bf16)
-    combine_high = (jnp.dot(spread, weights_high, preferred_element_type=f32) * chooser).T
-    combine_low = (jnp.dot(spread, weights_low, preferred_element_type=f32) * chooser).T
-    combine_high = combine_high.astype(bf16)
-    combine_low = combine_low.astype(bf16)
-    mid_ref[...] = mid_buf[core]
-
-    def relay(index, carry):
-        step = step_at(ep_count - 2 - index)
-        out_copy(step).wait_recv()
-        rows_copy(step).start()
-        return carry
-
-    lax.fori_loop(0, ep_count - 1, relay, 0)
-
-    def arrive(step, carry):
-        rows_arrival(step).wait_recv()
-        return carry
-
-    lax.fori_loop(0, ep_count, arrive, 0)
-
+    combine = jnp.dot(spread, weights.astype(bf16), preferred_element_type=f32) * chooser
+    combine = combine.T.astype(bf16)
+    for index in range(n_groups):
+        comb_own[index] = combine[:, index * block_rows : (index + 1) * block_rows]
+    comb_all[group] = comb_own[group]
+    each(1, n_groups, lambda block: across(block, *comb_args).start())
+
+    def relay_out(block):
+        across_arrival(block, *place_args).wait_recv()
+        across_arrival(block, *cross_args).wait_recv()
+        fan_out(block)
+
+    each(1, n_groups, relay_out)
     for load in loads[1:]:
         load.wait()
-    for index in range(n_blocks):
-        experts = slice(index * per_block, (index + 1) * per_block)
-        gate_part = jnp.zeros((block_rows, gate_ref.shape[1]), f32)
-        up_part = jnp.zeros((block_rows, gate_ref.shape[1]), f32)
+
+    def term_copy(block):
+        return remote(
+            term_send.at[block],
+            term_recv.at[block],
+            term_send_sems.at[block],
+            term_recv_sems.at[block],
+            (me, other),
+        )
+
+    def back_copy(block, step):
+        return remote(
+            result_buf.at[block, to_rank[step]],
+            back_buf.at[block, rank],
+            back_send_sems.at[block, step],
+            back_recv_sems.at[block, rank],
+            (base + to_rank[step], core),
+        )
+
+    def back_arrival(block, step):
+        return remote(
+            result_buf.at[block, to_rank[step]],
+            back_buf.at[block, from_rank[step]],
+            back_send_sems.at[block, step],
+            back_recv_sems.at[block, from_rank[step]],
+            (base + from_rank[step], core),
+        )
+
+    def experts(block):
+        first = source_group(block) * size
+        for step in reversed(steps):
+            fan_arrival(block, step).wait_recv()
+            rows_copy(first + from_rank[step]).start()
+        for index in range(size):
+            rows_arrival(first + index).wait_recv()
+        gate_part = jnp.zeros((block_rows, hidden_width), f32)
+        up_part = jnp.zeros((block_rows, hidden_width), f32)
         for piece in range(2):
             columns = slice(piece * half, (piece + 1) * half)
-            rows = rows_buf[piece, experts].reshape(block_rows, half)
+            rows = rows_buf[piece, pl.ds(first, size)].reshape(block_rows, half)
             gate_part += jnp.dot(rows, gate_ref[columns, :], preferred_element_type=f32)
             up_part += jnp.dot(rows, up_ref[columns, :], preferred_element_type=f32)
         hidden = (gate_part / (1.0 + jnp.exp(-gate_part)) * up_part).astype(bf16)
-        hidden_buf[experts] = hidden.reshape(per_block, cap, gate_ref.shape[1])
-
-    n_parts = term_send.shape[0]
-    per_part = ep_count // n_parts
-    first_part = me // per_part
-
-    def part_at(index):
-        return lax.rem(first_part + index + n_parts // 2, n_parts)
-
-    def term_copy(part):
-        return pair_copy(
-            term_send.at[part],
-            term_recv.at[part],
-            term_send_sems.at[part],
-            term_recv_sems.at[part],
-        )
-
-    def part_term(part, which):
-        hidden = hidden_buf[pl.ds(part * per_part, per_part)]
-        hidden = hidden.reshape(per_part * cap, gate_ref.shape[1])
-        term = jnp.dot(hidden, down_ref[which], preferred_element_type=f32)
-        return term.astype(bf16).reshape(per_part, cap, half)
-
-    def back_copy(peer):
-        return pltpu.make_async_remote_copy(
-            src_ref=result_buf.at[peer],
-            dst_ref=back_buf.at[me],
-            send_sem=back_send_sems.at[peer],
-            recv_sem=back_recv_sems.at[me],
-            device_id=(peer, core),
-            device_id_type=mesh_ids,
-        )
-
-    def back_arrival(peer):
-        return pltpu.make_async_remote_copy(
-            src_ref=result_buf.at[peer],
-            dst_ref=back_buf.at[peer],
-            send_sem=back_send_sems.at[peer],
-            recv_sem=back_recv_sems.at[peer],
-            device_id=(peer, core),
-            device_id_type=mesh_ids,
-        )
-
-    def send_terms(index, carry):
-        part = part_at(index)
-        term_send[part] = part_term(part, other)
-        term_copy(part).start()
-        return carry
-
-    lax.fori_loop(0, n_parts, send_terms, 0)
-
-    def own_terms(index, carry):
-        part = part_at(index)
-        term_own[part] = part_term(part, core)
-        return carry
-
-    lax.fori_loop(0, n_parts, own_terms, 0)
-
-    def finish_part(index, carry):
-        part = part_at(index)
-        term_copy(part).wait_recv()
-        total = term_own[part].astype(f32) + term_recv[part].astype(f32)
-        result_buf[pl.ds(part * per_part, per_part)] = total.astype(bf16)
-
-        def start_back(inner, carry_inner):
-            peer = part * per_part + inner
-
-            @pl.when(peer != me)
-            def _():
-                back_copy(peer).start()
-
-            return carry_inner
-
-        lax.fori_loop(0, per_part, start_back, 0)
-        return carry
-
-    lax.fori_loop(0, n_parts, finish_part, 0)
-    back_buf[me] = result_buf[me]
-
-    def finish_sends(step, carry):
-        out_copy(step).wait_send()
-        back_arrival(peer_at(step)).wait_recv()
-        back_copy(peer_at(step)).wait_send()
-        return carry
-
-    lax.fori_loop(1, ep_count, finish_sends, 0)
-
-    def finish_pair(step, carry):
-        rows_copy(step).wait_send()
-        return carry
-
-    lax.fori_loop(0, ep_count, finish_pair, 0)
-
-    def finish_terms(part, carry):
-        term_copy(part).wait_send()
-        return carry
-
-    lax.fori_loop(0, n_parts, finish_terms, 0)
-
-    back = back_buf[...].reshape(total_rows, half)
-    moe_out = jnp.dot(combine_high, back, preferred_element_type=f32)
-    moe_out += jnp.dot(combine_low, back, preferred_element_type=f32)
-    moe_ref[...] = moe_out
+        term_send[block] = jnp.dot(
+            hidden, down_ref[other], preferred_element_type=f32
+        ).astype(bf16)
+        term_copy(block).start()
+        term = jnp.dot(hidden, down_ref[core], preferred_element_type=f32).astype(bf16)
+        term_copy(block).wait_recv()
+        total = term.astype(f32) + term_recv[block].astype(f32)
+        result_buf[block] = total.astype(bf16).reshape(size, cap, half)
+        for step in steps:
+            back_copy(block, step).start()
+        back_buf[block, rank] = result_buf[block, rank]
+
+    each(0, n_groups, experts)
+
+    def gather(block):
+        for step in reversed(steps):
+            back_arrival(block, step).wait_recv()
+        back = back_buf[block].reshape(block_rows, half)
+        return jnp.dot(comb_all[source_group(block)], back, preferred_element_type=f32)
+
+    def sum_copy(block):
+        origin = source_group(block)
+        return remote(
+            sum_send.at[block],
+            sum_recv.at[group],
+            sum_send_sems.at[block],
+            sum_recv_sems.at[group],
+            (origin * size + rank, core),
+        )
+
+    def sum_arrival(block):
+        origin = source_group(block)
+        return remote(
+            sum_send.at[block],
+            sum_recv.at[origin],
+            sum_send_sems.at[block],
+            sum_recv_sems.at[origin],
+            (origin * size + rank, core),
+        )
+
+    def return_sum(block):
+        across_arrival(block, *comb_args).wait_recv()
+        sum_send[block] = gather(block).astype(bf16)
+        sum_copy(block).start()
+
+    each(1, n_groups, return_sum)
+    part_buf[0] = mid_buf[core].astype(f32) + gather(0)
+
+    def finish_sends(block):
+        for step in steps:
+            fan_copy(block, step).wait_send()
+            back_copy(block, step).wait_send()
+        for index in range(size):
+            rows_copy(source_group(block) * size + index).wait_send()
+        term_copy(block).wait_send()
+
+    each(0, n_groups, finish_sends)
+
+    def finish_cross(block):
+        across(block, *place_args).wait_send()
+        across(block, *comb_args).wait_send()
+        across(block, *cross_args).wait_send()
+        sum_copy(block).wait_send()
+        sum_arrival(block).wait_recv()
+        part_buf[0] += sum_recv[source_group(block)].astype(f32)
+
+    each(1, n_groups, finish_cross)
+    out_ref[...] = part_buf[0].astype(bf16)
 
 
 def shards(
@@ -525,18 +581,15 @@
     half_width = width_model // tp_count
     limit = max(2, 2 * seq_count * top_count // ep_count)
     cap = -(-limit // 16) * 16
-    block_rows = min(ep_count * cap, 256)
-    n_parts = min(4, ep_count)
-    per_part = ep_count // n_parts
+    n_groups = router_group.shape[1]
+    size = ep_count // n_groups
+    block_rows = size * cap
     hidden_width = expert_gate.shape[2]
-    moe_out, mid_half = pl.pallas_call(
-        functools.partial(moe_kernel, ep_count, block_rows),
-        out_shape=(
-            jax.ShapeDtypeStruct((seq_count, half_width), f32),
-            jax.ShapeDtypeStruct((seq_count, half_width), bf16),
-        ),
+    layer_out = pl.pallas_call(
+        functools.partial(moe_kernel, ep_count),
+        out_shape=jax.ShapeDtypeStruct((seq_count, half_width), bf16),
         in_specs=[vmem, anywhere] + [vmem] * 5 + [anywhere] * 3,
-        out_specs=(vmem, vmem),
+        out_specs=vmem,
         scratch_shapes=[
             pltpu.VMEM((width_model, hidden_width), bf16),
             pltpu.VMEM((width_model, hidden_width), bf16),
@@ -546,23 +599,37 @@
             pltpu.VMEM((tp_count, seq_count, half_width), f32),
             pltpu.VMEM((tp_count, seq_count, half_width), bf16),
             pltpu.VMEM((tp_count, seq_count, half_width), bf16),
-            pltpu.VMEM((ep_count, cap, half_width), bf16),
+            pltpu.VMEM((n_groups, block_rows, seq_count), bf16),
+            pltpu.VMEM((n_groups, block_rows, seq_count), bf16),
+            pltpu.VMEM((n_groups, seq_count, block_rows), bf16),
+            pltpu.VMEM((n_groups, seq_count, block_rows), bf16),
+            pltpu.VMEM((seq_count, half_width), bf16),
+            pltpu.VMEM((n_groups, seq_count, half_width), bf16),
+            pltpu.VMEM((n_groups, size, cap, half_width), bf16),
             pltpu.VMEM((tp_count, ep_count, cap, half_width), bf16),
-            pltpu.VMEM((ep_count, cap, hidden_width), bf16),
-            pltpu.VMEM((n_parts, per_part, cap, half_width), bf16),
-            pltpu.VMEM((n_parts, per_part, cap, half_width), bf16),
-            pltpu.VMEM((n_parts, per_part, cap, half_width), bf16),
-            pltpu.VMEM((ep_count, cap, half_width), bf16),
-            pltpu.VMEM((ep_count, cap, half_width), bf16),
+            pltpu.VMEM((n_groups, block_rows, half_width), bf16),
+            pltpu.VMEM((n_groups, block_rows, half_width), bf16),
+            pltpu.VMEM((n_groups, size, cap, half_width), bf16),
+            pltpu.VMEM((n_groups, size, cap, half_width), bf16),
+            pltpu.VMEM((n_groups, seq_count, half_width), bf16),
+            pltpu.VMEM((n_groups, seq_count, half_width), bf16),
             dma((2,)),
+            dma((n_groups,)),
+            dma((n_groups,)),
+            dma((n_groups,)),
+            dma((n_groups,)),
+            dma((n_groups,)),
+            dma((n_groups,)),
+            dma((n_groups, size)),
             dma((ep_count,)),
             dma((ep_count,)),
             dma((ep_count,)),
-            dma((ep_count,)),
-            dma((n_parts,)),
-            dma((n_parts,)),
-            dma((ep_count,)),
-            dma((ep_count,)),
+            dma((n_groups,)),
+            dma((n_groups,)),
+            dma((n_groups, size)),
+            dma((n_groups, size)),
+            dma((n_groups,)),
+            dma((n_groups,)),
             dma((5,)),
         ],
         compiler_params=pltpu.CompilerParams(
@@ -580,7 +647,6 @@
         expert_up,
         expert_down,
     )
-    layer_out = (mid_half.astype(f32) + moe_out).astype(bf16)
     return (layer_out, state_out)
 
 

time: 49.7 us -> 42.5 us (0.86)
  Pallas kernels: 47.3 us -> 40.1 us
  other arithmetic: 1.55 us -> 0 us
  local copies, waits for them, and re-layouts: 0 us -> 1.47 us
    pallas_call x1, Pallas kernels: 39.5 us -> 32.4 us  [shards(): pl.pallas_call(functools.partial(moe_kernel, ep_count), out_shape=jax.Sha...]
    convert_element_type x1 -> x0, other arithmetic: 1.55 us -> none  [shards(): layer_out = (mid_half.astype(f32) + moe_out).astype(bf16)]
    unnamed x0 -> x1, local copies, waits for them, and re-layouts: none -> 1.47 us
where the time goes in v2:
time: 42.5 us; the launch traced here: 42.3 us
  Pallas kernels  40.1 us (94%)
  local copies, waits for them, and re-layouts  1.47 us (3%)
  between operations  0.65 us (2%)
    pallas_call x1, Pallas kernels, shards(): pl.pallas_call(functools.partial(moe_kernel, ep_count), out_shape=jax.Sha...  32.4 us
    pallas_call x1, Pallas kernels, shards(): pl.pallas_call(mixer_kernel, out_shape=(jax.ShapeDtypeStruct((seq_count,...  7.78 us
    unnamed x1, local copies, waits for them, and re-layouts  1.47 us

profile of v2, /device:TPU:0, one launch (start us, length us, event | category | flops | bytes accessed | tf_op | source)
XLA Modules:
  0.0 42.3 jit_solution(7500667397587645360)
XLA Ops:
  0.6 7.8 %shard_map.221 = (bf16[32,256]{1,0:T(8,128)(2,1)}, f32[32,4,64,64]{3,2,1,0:T(8,128)}) custom-call(bf16[32,2048]{1,0:T(8,128)(2,1)} %tokens_ref.3, bf16[2048]{0:T(1024)(128)(2,1)} %norm_ref.2, bf16[2048,256]{1,0:T(8,128)(2,1)} %w_recept_hbm.1, bf16[2048,256]{1,0:T(8,128)(2,1)} %w_key_hbm.1, bf16[2048,256]{1,0:T(8,128)(2,1)} %w_value_hbm.1, ...), custom_call_target="tpu_custom_call" | custom-call | tf_op jit(solution)/shard_map/pallas_call | solution.py:547
  8.4 32.4 %shard_map.222 = bf16[32,1024]{1,0:T(8,128)(2,1)} custom-call(bf16[32,256]{1,0:T(8,128)(2,1)} %get-tuple-element.4.mixed_ref, bf16[256,2048]{1,0:T(8,128)(2,1)} %w_out_hbm.1, bf16[32,2048]{1,0:T(8,128)(2,1)} %tokens_ref.3, bf16[2048]{0:T(1024)(128)(2,1)} %norm_ref.3, bf16[2,2048]{1,0:T(2,128)(2,1)} %bitcast.8, bf16[16,2048]{1,0:T(8,128)(2,1)} %bitcast.7, ...), custom_call_target="tpu_custom_call" | custom-call | tf_op jit(solution)/shard_map/pallas_call | solution.py:588
  40.8 1.5 %copy.25 = bf16[32,1024]{1,0:T(8,128)(2,1)} copy(bf16[32,1024]{1,0:T(8,128)(2,1)} %shard_map.222) | data formatting | bytes 131072

commit v3 on v2

--- a/solution.py
+++ b/solution.py
@@ -8,116 +8,23 @@
 from jax.sharding import PartitionSpec as P
 
 
-def mixer_kernel(
-    tokens_ref, norm_ref, w_recept_hbm, w_key_hbm, w_value_hbm, decay_down_ref, decay_up_ref, decay_base_ref,
-    iclr_down_ref, iclr_up_ref, iclr_base_ref, key_scale_ref, key_mix_ref, state_hbm,
-    mixed_ref, state_out_hbm,
-    weights, state_buf, out_buf, weight_sems, in_sems, out_sems,
-):
-    f32 = jnp.float32
-    bf16 = jnp.bfloat16
-    seq_count, width = tokens_ref.shape
-    heads, head_size = state_hbm.shape[1], state_hbm.shape[3]
-    channels = heads * head_size
-    n_chunks = in_sems.shape[0]
-    per_chunk = seq_count // n_chunks
-    rows_dims = (((1,), (1,)), ((), ()))
-    weight_loads = [
-        pltpu.make_async_copy(source, weights.at[index], weight_sems.at[index])
-        for index, source in enumerate((w_key_hbm, w_recept_hbm, w_value_hbm))
-    ]
-    for load in weight_loads:
-        load.start()
-    state_loads = []
-    state_stores = []
-    for index in range(n_chunks):
-        span = pl.ds(index * per_chunk, per_chunk)
-        state_loads.append(
-            pltpu.make_async_copy(state_hbm.at[span], state_buf.at[span], in_sems.at[index])
-        )
-        state_stores.append(
-            pltpu.make_async_copy(out_buf.at[span], state_out_hbm.at[span], out_sems.at[index])
-        )
-        state_loads[index].start()
-
-    tokens = tokens_ref[...].astype(f32)
-    factor = lax.rsqrt(jnp.mean(tokens * tokens, axis=1, keepdims=True) + 1e-06)
-    normed = (tokens * factor * norm_ref[...].reshape(1, width).astype(f32)).astype(bf16)
-    decay_low = jnp.tanh(
-        lax.dot_general(normed, decay_down_ref[...], rows_dims, preferred_element_type=f32)
-    ).astype(bf16)
-    iclr_low = lax.dot_general(
-        normed, iclr_down_ref[...], rows_dims, preferred_element_type=f32
-    ).astype(bf16)
-    decay_in = decay_base_ref[...].reshape(1, channels) + jnp.dot(
-        decay_low, decay_up_ref[...], preferred_element_type=f32
-    )
-    decays = jnp.exp(-jnp.exp(jnp.float32(-0.5)) * jax.nn.sigmoid(decay_in))
-    rate = jax.nn.sigmoid(
-        iclr_base_ref[...].reshape(1, channels)
-        + jnp.dot(iclr_low, iclr_up_ref[...], preferred_element_type=f32)
-    )
-
-    def project(index):
-        weight_loads[index].wait()
-        rows = jnp.dot(normed, weights[index], preferred_element_type=f32)
-        return rows.astype(bf16).astype(f32)
-
-    key = project(0)
-    scaled = key * key_scale_ref[...].reshape(1, channels).astype(f32)
-    key_mod = key * (1.0 + (rate - 1.0) * key_mix_ref[...].reshape(1, channels).astype(f32))
-    spans = [slice(head * head_size, (head + 1) * head_size) for head in range(heads)]
-    units = []
-    for span in spans:
-        part = scaled[:, span]
-        units.append(part * lax.rsqrt(jnp.sum(part * part, axis=1, keepdims=True) + 1e-06))
-    recept = project(1)
-    readers, writers, gains = [], [], []
-    for head, span in enumerate(spans):
-        unit, query = units[head], recept[:, span]
-        drop = unit * rate[:, span]
-        shift = jnp.sum(drop * query, axis=1, keepdims=True)
-        gains.append(jnp.sum(key_mod[:, span] * query, axis=1, keepdims=True))
-        reader = decays[:, span] * query - unit * shift
-        readers.append(jnp.concatenate([unit, reader], axis=0).astype(bf16))
-        writers.append(jnp.concatenate([-drop, key_mod[:, span]], axis=0).astype(bf16))
-    value = project(2)
-    value_t = jnp.concatenate([value, value], axis=0).T
-
-    lanes = lax.broadcasted_iota(jnp.int32, (per_chunk, head_size, 2 * seq_count), 2)
-    seqs = lax.broadcasted_iota(jnp.int32, (per_chunk, head_size, 2 * seq_count), 0)
-    first = lanes < seq_count
-    owner = jnp.where(first, lanes, lanes - seq_count)
-    totals = [jnp.zeros((head_size, 2 * seq_count), f32) for _ in range(heads)]
-    for index in range(n_chunks):
-        rows = slice(index * per_chunk, (index + 1) * per_chunk)
-        here = owner == seqs + index * per_chunk
-        state_loads[index].wait()
-        for head, span in enumerate(spans):
-            state = state_buf[rows, head]
-            flat = state.reshape(per_chunk * head_size, head_size).astype(bf16)
-            read = lax.dot_general(flat, readers[head], rows_dims, preferred_element_type=f32)
-            read = read.reshape(per_chunk, head_size, 2 * seq_count)
-            totals[head] += jnp.sum(jnp.where(here, read, 0.0), axis=0)
-            terms = jnp.where(here, jnp.where(first, read, value_t[span, :][None]), 0.0)
-            terms = terms.reshape(per_chunk * head_size, 2 * seq_count).astype(bf16)
-            change = jnp.dot(terms, writers[head], preferred_element_type=f32)
-            out_buf[rows, head] = state * decays[rows, span][:, None, :] + change.reshape(
-                per_chunk, head_size, head_size
-            )
-        state_stores[index].start()
-    total = jnp.concatenate(totals, axis=0).T[seq_count:]
-    for head, span in enumerate(spans):
-        mixed_ref[:, span] = (total[:, span] + value[:, span] * gains[head]).astype(bf16)
-    for store in state_stores:
-        store.wait()
-
-
-def moe_kernel(
+def layer_kernel(
     ep_count,
-    mixed_ref,
+    tokens_ref,
+    norm_mix_ref,
+    w_recept_hbm,
+    w_key_hbm,
+    w_value_hbm,
+    decay_down_ref,
+    decay_up_ref,
+    decay_base_ref,
+    iclr_down_ref,
+    iclr_up_ref,
+    iclr_base_ref,
+    key_scale_ref,
+    key_mix_ref,
+    state_hbm,
     w_out_hbm,
-    tokens_ref,
     norm_ref,
     router_group_ref,
     router_expert_ref,
@@ -126,6 +33,12 @@
     up_hbm,
     down_hbm,
     out_ref,
+    state_out_ref,
+    weights,
+    state_buf,
+    terms_buf,
+    decay_buf,
+    writer_buf,
     gate_ref,
     up_ref,
     down_ref,
@@ -166,6 +79,8 @@
     sum_send_sems,
     sum_recv_sems,
     load_sems,
+    weight_sems,
+    in_sems,
 ):
     f32 = jnp.float32
     bf16 = jnp.bfloat16
@@ -174,6 +89,9 @@
     other = 1 - core
     seq_count, width = tokens_ref.shape
     half = width // 2
+    heads, head_size = state_hbm.shape[1], state_hbm.shape[3]
+    channels = heads * head_size
+    rows_dims = (((1,), (1,)), ((), ()))
     cap = send_buf.shape[2]
     total_rows = ep_count * cap
     mesh_ids = pl.DeviceIdType.MESH
@@ -239,8 +157,90 @@
         pltpu.make_async_copy(down_hbm.at[0, :, pl.ds(0, half)], down_ref.at[0], load_sems.at[3]),
         pltpu.make_async_copy(down_hbm.at[0, :, pl.ds(half, half)], down_ref.at[1], load_sems.at[4]),
     ]
+    weight_loads = [
+        pltpu.make_async_copy(source, weights.at[index], weight_sems.at[index])
+        for index, source in enumerate((w_key_hbm, w_recept_hbm, w_value_hbm))
+    ]
+    for load in weight_loads:
+        load.start()
+    n_chunks = in_sems.shape[0]
+    per_chunk = seq_count // n_chunks
+    state_loads = []
+    for index in range(n_chunks):
+        span = pl.ds(index * per_chunk, per_chunk)
+        state_loads.append(
+            pltpu.make_async_copy(state_hbm.at[span], state_buf.at[span], in_sems.at[index])
+        )
+        state_loads[index].start()
     for load in loads:
         load.start()
+
+    tokens = tokens_ref[...].astype(f32)
+    factor = lax.rsqrt(jnp.mean(tokens * tokens, axis=1, keepdims=True) + 1e-06)
+    normed = (tokens * factor * norm_mix_ref[...].reshape(1, width).astype(f32)).astype(bf16)
+    decay_low = jnp.tanh(
+        lax.dot_general(normed, decay_down_ref[...], rows_dims, preferred_element_type=f32)
+    ).astype(bf16)
+    iclr_low = lax.dot_general(
+        normed, iclr_down_ref[...], rows_dims, preferred_element_type=f32
+    ).astype(bf16)
+    decay_in = decay_base_ref[...].reshape(1, channels) + jnp.dot(
+        decay_low, decay_up_ref[...], preferred_element_type=f32
+    )
+    decays = jnp.exp(-jnp.exp(jnp.float32(-0.5)) * jax.nn.sigmoid(decay_in))
+    rate = jax.nn.sigmoid(
+        iclr_base_ref[...].reshape(1, channels)
+        + jnp.dot(iclr_low, iclr_up_ref[...], preferred_element_type=f32)
+    )
+
+    def project(index):
+        weight_loads[index].wait()
+        rows = jnp.dot(normed, weights[index], preferred_element_type=f32)
+        return rows.astype(bf16).astype(f32)
+
+    key = project(0)
+    scaled = key * key_scale_ref[...].reshape(1, channels).astype(f32)
+    key_mod = key * (1.0 + (rate - 1.0) * key_mix_ref[...].reshape(1, channels).astype(f32))
+    spans = [slice(head * head_size, (head + 1) * head_size) for head in range(heads)]
+    units = []
+    for span in spans:
+        part = scaled[:, span]
+        units.append(part * lax.rsqrt(jnp.sum(part * part, axis=1, keepdims=True) + 1e-06))
+    recept = project(1)
+    readers, writers, gains = [], [], []
+    for head, span in enumerate(spans):
+        unit, query = units[head], recept[:, span]
+        drop = unit * rate[:, span]
+        shift = jnp.sum(drop * query, axis=1, keepdims=True)
+        gains.append(jnp.sum(key_mod[:, span] * query, axis=1, keepdims=True))
+        reader = decays[:, span] * query - unit * shift
+        readers.append(jnp.concatenate([unit, reader], axis=0).astype(bf16))
+        writers.append(jnp.concatenate([-drop, key_mod[:, span]], axis=0).astype(bf16))
+    value = project(2)
+    value_t = jnp.concatenate([value, value], axis=0).T
+
+    lanes = lax.broadcasted_iota(jnp.int32, (per_chunk, head_size, 2 * seq_count), 2)
+    seqs = lax.broadcasted_iota(jnp.int32, (per_chunk, head_size, 2 * seq_count), 0)
+    first = lanes < seq_count
+    owner = jnp.where(first, lanes, lanes - seq_count)
+    totals = [jnp.zeros((head_size, 2 * seq_count), f32) for _ in range(heads)]
+    for index in range(n_chunks):
+        rows = slice(index * per_chunk, (index + 1) * per_chunk)
+        here = owner == seqs + index * per_chunk
+        state_loads[index].wait()
+        for head, span in enumerate(spans):
+            flat = state_buf[rows, head].reshape(per_chunk * head_size, head_size).astype(bf16)
+            read = lax.dot_general(flat, readers[head], rows_dims, preferred_element_type=f32)
+            read = read.reshape(per_chunk, head_size, 2 * seq_count)
+            totals[head] += jnp.sum(jnp.where(here, read, 0.0), axis=0)
+            terms = jnp.where(here, jnp.where(first, read, value_t[span, :][None]), 0.0)
+            terms_buf[head, rows] = terms.astype(bf16)
+    total = jnp.concatenate(totals, axis=0).T[seq_count:]
+    mixed = [total[:, span] + value[:, span] * gains[head] for head, span in enumerate(spans)]
+    mixed = jnp.concatenate(mixed, axis=1).astype(bf16)
+    for head, span in enumerate(spans):
+        decay_buf[head] = decays[:, span]
+        writer_buf[head] = writers[head]
 
     expert_ids = lax.broadcasted_iota(jnp.int32, (ep_count, seq_count), 0)
     uses = jnp.zeros((ep_count, seq_count), f32)
@@ -266,7 +266,7 @@
     for index in range(2):
         columns = slice(index * half, (index + 1) * half)
         part_buf[index] = jnp.dot(
-            mixed_ref[...], w_out_ref[:, columns], preferred_element_type=f32
+            mixed, w_out_ref[:, columns], preferred_element_type=f32
         )
     pl.semaphore_wait(barrier, (n_groups - 1) + (size - 1) + 1)
 
@@ -367,7 +367,6 @@
 
     fan_out(0)
 
-    rows_dims = (((1,), (1,)), ((), ()))
     group_logit = jnp.zeros(group_hit.shape, f32)
     expert_logit = jnp.zeros(uses.shape, f32)
     for index in range(2):
@@ -380,13 +379,25 @@
         )
     group_prob = jax.nn.sigmoid(jnp.sum(group_logit * group_hit, axis=0, keepdims=True))
     scores = jax.nn.sigmoid(expert_logit) * uses
-    weights = group_prob * scores / jnp.sum(scores, axis=0, keepdims=True)
-    combine = jnp.dot(spread, weights.astype(bf16), preferred_element_type=f32) * chooser
+    route_weights = group_prob * scores / jnp.sum(scores, axis=0, keepdims=True)
+    combine = jnp.dot(spread, route_weights.astype(bf16), preferred_element_type=f32) * chooser
     combine = combine.T.astype(bf16)
     for index in range(n_groups):
         comb_own[index] = combine[:, index * block_rows : (index + 1) * block_rows]
     comb_all[group] = comb_own[group]
     each(1, n_groups, lambda block: across(block, *comb_args).start())
+
+    def update_state():
+        for index in range(n_chunks):
+            rows = slice(index * per_chunk, (index + 1) * per_chunk)
+            for head in range(heads):
+                terms = terms_buf[head, rows].reshape(per_chunk * head_size, 2 * seq_count)
+                change = jnp.dot(terms, writer_buf[head], preferred_element_type=f32)
+                state_out_ref[rows, head] = state_buf[rows, head] * decay_buf[head, rows][
+                    :, None, :
+                ] + change.reshape(per_chunk, head_size, head_size)
+
+    update_state()
 
     def relay_out(block):
         across_arrival(block, *place_args).wait_recv()
@@ -544,39 +555,6 @@
     vmem = pl.BlockSpec(memory_space=pltpu.VMEM)
     anywhere = pl.BlockSpec(memory_space=pl.ANY)
     n_chunks = 2 if seq_count % 2 == 0 else 1
-    mixed, state_out = pl.pallas_call(
-        mixer_kernel,
-        out_shape=(
-            jax.ShapeDtypeStruct((seq_count, channels), bf16),
-            jax.ShapeDtypeStruct(state_in.shape, f32),
-        ),
-        in_specs=[vmem] * 2 + [anywhere] * 3 + [vmem] * 8 + [anywhere],
-        out_specs=(vmem, anywhere),
-        scratch_shapes=[
-            pltpu.VMEM((3, width_model, channels), bf16),
-            pltpu.VMEM(state_in.shape, f32),
-            pltpu.VMEM(state_in.shape, f32),
-            dma((3,)),
-            dma((n_chunks,)),
-            dma((n_chunks,)),
-        ],
-        compiler_params=pltpu.CompilerParams(vmem_limit_bytes=60 * 1024 * 1024),
-    )(
-        tokens_in,
-        norm_mix,
-        w_recept,
-        w_key,
-        w_value,
-        decay_down.T,
-        decay_up,
-        decay_base,
-        iclr_down.T,
-        iclr_up,
-        iclr_base,
-        key_scale,
-        key_mix,
-        state_in,
-    )
     top_count = routes.shape[1]
     half_width = width_model // tp_count
     limit = max(2, 2 * seq_count * top_count // ep_count)
@@ -585,12 +563,27 @@
     size = ep_count // n_groups
     block_rows = size * cap
     hidden_width = expert_gate.shape[2]
-    layer_out = pl.pallas_call(
-        functools.partial(moe_kernel, ep_count),
-        out_shape=jax.ShapeDtypeStruct((seq_count, half_width), bf16),
-        in_specs=[vmem, anywhere] + [vmem] * 5 + [anywhere] * 3,
-        out_specs=vmem,
+    block_bytes = ep_count * cap * width_model
+    vmem_limit = min(58 * 1024 * 1024, 24 * 1024 * 1024 + 10 * block_bytes)
+    layer = pl.pallas_call(
+        functools.partial(layer_kernel, ep_count),
+        out_shape=(
+            jax.ShapeDtypeStruct((seq_count, half_width), bf16),
+            jax.ShapeDtypeStruct(state_in.shape, f32),
+        ),
+        in_specs=[vmem] * 2
+        + [anywhere] * 3
+        + [vmem] * 8
+        + [anywhere] * 2
+        + [vmem] * 4
+        + [anywhere] * 3,
+        out_specs=(vmem, vmem),
         scratch_shapes=[
+            pltpu.VMEM((3, width_model, channels), bf16),
+            pltpu.VMEM(state_in.shape, f32),
+            pltpu.VMEM((heads_here, seq_count, head_size, 2 * seq_count), bf16),
+            pltpu.VMEM((heads_here, seq_count, head_size), f32),
+            pltpu.VMEM((heads_here, 2 * seq_count, head_size), bf16),
             pltpu.VMEM((width_model, hidden_width), bf16),
             pltpu.VMEM((width_model, hidden_width), bf16),
             pltpu.VMEM((tp_count, hidden_width, half_width), bf16),
@@ -631,21 +624,20 @@
             dma((n_groups,)),
             dma((n_groups,)),
             dma((5,)),
+            dma((3,)),
+            dma((n_chunks,)),
         ],
         compiler_params=pltpu.CompilerParams(
-            collective_id=0, has_side_effects=True, vmem_limit_bytes=60 * 1024 * 1024
+            collective_id=0, has_side_effects=True, vmem_limit_bytes=vmem_limit
         ),
-    )(
-        mixed,
-        w_out,
-        tokens_in,
-        norm_moe,
-        router_group.T,
-        router_expert.T,
-        routes.T,
-        expert_gate,
-        expert_up,
-        expert_down,
+    )
+    operands = (
+        tokens_in, norm_mix, w_recept, w_key, w_value, decay_down.T, decay_up, decay_base,
+        iclr_down.T, iclr_up, iclr_base, key_scale, key_mix, state_in, w_out, norm_moe,
+        router_group.T, router_expert.T, routes.T, expert_gate, expert_up, expert_down,
+    )
+    layer_out, state_out = layer(
+        *(pltpu.with_memory_space_constraint(operand, pltpu.HBM) for operand in operands)
     )
     return (layer_out, state_out)
 

time: 42.5 us -> 39.3 us (0.925)
  Pallas kernels: 40.1 us -> 35.9 us
  local copies, waits for them, and re-layouts: 1.47 us -> 2.64 us
    pallas_call x2 -> x1, Pallas kernels: 40.1 us -> 35.9 us  [shards(): layer(*(pltpu.with_memory_space_constraint(operand, pltpu.HBM) for operan...]
    unnamed x1 -> x2, local copies, waits for them, and re-layouts: 1.47 us -> 2.64 us
where the time goes in v3:
time: 39.3 us; the launch traced here: 39.2 us
  Pallas kernels  35.9 us (91%)
  local copies, waits for them, and re-layouts  2.64 us (7%)
  between operations  0.65 us (2%)
    pallas_call x1, Pallas kernels, shards(): layer(*(pltpu.with_memory_space_constraint(operand, pltpu.HBM) for operan...  35.9 us
    unnamed x2, local copies, waits for them, and re-layouts  2.64 us

profile of v3, /device:TPU:0, one launch (start us, length us, event | category | flops | bytes accessed | tf_op | source)
XLA Modules:
  0.0 39.2 jit_solution(5819297297679889896)
XLA Ops:
  0.6 35.9 %shard_map.221 = (bf16[32,1024]{1,0:T(8,128)(2,1)S(1)}, f32[32,4,64,64]{3,2,1,0:T(8,128)S(1)}) custom-call(bf16[32,2048]{1,0:T(8,128)(2,1)} %tokens_ref.1, bf16[2048]{0:T(1024)(128)(2,1)} %norm_mix_ref.1, bf16[2048,256]{1,0:T(8,128)(2,1)} %w_recept_hbm.1, bf16[2048,256]{1,0:T(8,128)(2,1)} %w_key_hbm.1, bf16[2048,256]{1,0:T(8,128)(2,1)} %w_value_hbm.1, ...), custom_call_target="tpu_custom_call" | custom-call | tf_op jit(solution)/shard_map/pallas_call | solution.py:639
  36.5 0.6 %copy.26 = bf16[32,1024]{1,0:T(8,128)(2,1)} copy(bf16[32,1024]{1,0:T(8,128)(2,1)S(1)} %get-tuple-element.4) | data formatting | bytes 131072
  37.2 2.0 %copy.27 = f32[32,4,64,64]{3,2,1,0:T(8,128)} copy(f32[32,4,64,64]{3,2,1,0:T(8,128)S(1)} %get-tuple-element.5) | data formatting | bytes 4194304

commit v4 on v3

v4 whole, which is shorter than its diff:
```python
import functools

import jax
import jax.numpy as jnp
from jax import lax
from jax.experimental import pallas as pl
from jax.experimental.pallas import tpu as pltpu
from jax.sharding import PartitionSpec as P


def layer_kernel(
    ep_count,
    tokens_hbm,
    routes_hbm,
    norm_mix_hbm,
    decay_down_hbm,
    iclr_down_hbm,
    decay_up_hbm,
    decay_base_hbm,
    iclr_up_hbm,
    iclr_base_hbm,
    key_scale_hbm,
    key_mix_hbm,
    norm_moe_hbm,
    router_group_hbm,
    router_expert_hbm,
    w_recept_hbm,
    w_key_hbm,
    w_value_hbm,
    state_hbm,
    w_out_hbm,
    gate_hbm,
    up_hbm,
    down_hbm,
    out_ref,
    state_out_ref,
    tokens_ref,
    routes_ref,
    norm_mix_ref,
    decay_down_ref,
    iclr_down_ref,
    decay_up_ref,
    decay_base_ref,
    iclr_up_ref,
    iclr_base_ref,
    key_scale_ref,
    key_mix_ref,
    norm_ref,
    router_group_ref,
    router_expert_ref,
    weights,
    state_buf,
    terms_buf,
    decay_buf,
    writer_buf,
    w_out_ref,
    first_ref,
    down_ref,
    part_buf,
    part_recv,
    mid_buf,
    norm_buf,
    place_own,
    place_all,
    comb_own,
    comb_all,
    rows_own,
    rows_all,
    send_buf,
    rows_buf,
    sums_own,
    sums_recv,
    result_buf,
    back_buf,
    total_send,
    total_recv,
    small_sems,
    weight_sems,
    in_sems,
    load_sems,
    share_send_sems,
    share_recv_sems,
    part_sems,
    place_send_sems,
    place_recv_sems,
    comb_send_sems,
    comb_recv_sems,
    cross_send_sems,
    cross_recv_sems,
    fan_send_sems,
    fan_recv_sems,
    sums_send_sems,
    sums_recv_sems,
    back_send_sems,
    back_recv_sems,
    total_send_sems,
    total_recv_sems,
):
    f32 = jnp.float32
    bf16 = jnp.bfloat16
    me = lax.axis_index("ep")
    core = lax.axis_index("tp")
    other = 1 - core
    seq_count, width = tokens_ref.shape
    half = width // 2
    heads, head_size = state_hbm.shape[1], state_hbm.shape[3]
    channels = heads * head_size
    rows_dims = (((1,), (1,)), ((), ()))
    cap = send_buf.shape[2]
    total_rows = ep_count * cap
    mesh_ids = pl.DeviceIdType.MESH
    n_groups = router_group_ref.shape[0]
    size = ep_count // n_groups
    group = me // size
    rank = me % size
    base = group * size
    block_rows = size * cap
    hidden_part = gate_hbm.shape[2]
    hidden_width = 2 * hidden_part
    power = size & (size - 1) == 0
    steps = sorted(range(1, size), key=lambda step: -bin(step).count("1"))
    near = [step for step in steps if 2 * step < size]
    far = [step for step in steps if 2 * step >= size]

    def flip(step):
        moved = rank * 0
        bit = 1
        while bit < size:
            value = rank // bit % 2
            moved = moved + bit * ((1 - value) if step & bit else value)
            bit *= 2
        return moved

    to_rank = {s: flip(s) if power else (rank + s) % size for s in steps}
    from_rank = {s: flip(s) if power else (rank + size - s) % size for s in steps}

    def each(low, high, visit):
        if high - low <= 2:
            for index in range(low, high):
                visit(index)
        else:
            lax.fori_loop(low, high, lambda index, carry: (visit(index), carry)[1], 0)

    def source_group(block):
        return (group + n_groups - block) % n_groups

    def target_group(block):
        return (group + block) % n_groups

    def remote(source, target, send_sem, recv_sem, device):
        return pltpu.make_async_remote_copy(
            src_ref=source,
            dst_ref=target,
            send_sem=send_sem,
            recv_sem=recv_sem,
            device_id=device,
            device_id_type=mesh_ids,
        )

    partner = (me, other)
    barrier = pltpu.get_barrier_semaphore()

    def greet(device):
        pl.semaphore_signal(barrier, inc=1, device_id=device, device_id_type=mesh_ids)

    each(1, n_groups, lambda block: greet((target_group(block) * size + rank, core)))
    for step in steps:
        greet((base + to_rank[step], core))
    greet(partner)

    small = [
        pltpu.make_async_copy(source, target, small_sems.at[index])
        for index, (source, target) in enumerate(
            (
                (tokens_hbm, tokens_ref),
                (routes_hbm, routes_ref),
                (norm_mix_hbm, norm_mix_ref),
                (decay_down_hbm, decay_down_ref),
                (iclr_down_hbm, iclr_down_ref),
                (decay_up_hbm, decay_up_ref),
                (decay_base_hbm, decay_base_ref),
                (iclr_up_hbm, iclr_up_ref),
                (iclr_base_hbm, iclr_base_ref),
                (key_scale_hbm, key_scale_ref),
                (key_mix_hbm, key_mix_ref),
                (norm_moe_hbm, norm_ref),
                (router_group_hbm, router_group_ref),
                (router_expert_hbm, router_expert_ref),
            )
        )
    ]
    for load in small:
        load.start()
    weight_loads = [
        pltpu.make_async_copy(source, weights.at[index], weight_sems.at[index])
        for index, source in enumerate((w_key_hbm, w_recept_hbm, w_value_hbm))
    ]
    for load in weight_loads:
        load.start()
    n_chunks = in_sems.shape[0]
    per_chunk = seq_count // n_chunks
    state_loads = []
    for index in range(n_chunks):
        span = pl.ds(index * per_chunk, per_chunk)
        state_loads.append(
            pltpu.make_async_copy(state_hbm.at[span], state_buf.at[span], in_sems.at[index])
        )

    def columns_of(which):
        return pl.ds(pl.multiple_of(which * half, half), half)

    hidden_here = pl.ds(pl.multiple_of(core * hidden_part, hidden_part), hidden_part)
    shared = (
        (lambda which: gate_hbm.at[0, columns_of(which)], first_ref.at[0, :, hidden_here]),
        (lambda which: up_hbm.at[0, columns_of(which)], first_ref.at[1, :, hidden_here]),
        (lambda which: down_hbm.at[0, :, columns_of(which)], down_ref.at[hidden_here]),
    )
    loads = [pltpu.make_async_copy(w_out_hbm, w_out_ref, load_sems.at[0])]
    shares = []
    for index, (source, target) in enumerate(shared):
        loads.append(pltpu.make_async_copy(source(core), target, load_sems.at[1 + index]))
        shares.append(
            remote(
                source(other), target, share_send_sems.at[index], share_recv_sems.at[index], partner
            )
        )
    for load in small[:2]:
        load.wait()

    expert_ids = lax.broadcasted_iota(jnp.int32, (ep_count, seq_count), 0)
    uses = jnp.zeros((ep_count, seq_count), f32)
    for index in range(routes_ref.shape[0]):
        uses += jnp.where(routes_ref[index : index + 1, :] == expert_ids, 1.0, 0.0)
    group_ids = lax.broadcasted_iota(jnp.int32, (n_groups, seq_count), 0)
    group_hit = jnp.where(routes_ref[0:1, :] // size == group_ids, 1.0, 0.0)
    row_ids = lax.broadcasted_iota(jnp.int32, (seq_count, seq_count), 0)
    column_ids = lax.broadcasted_iota(jnp.int32, (seq_count, seq_count), 1)
    earlier = jnp.where(row_ids < column_ids, 1.0, 0.0).astype(bf16)
    position = jnp.dot(uses.astype(bf16), earlier, preferred_element_type=f32)
    slots = jnp.where(uses > 0.5, position, -1.0).astype(bf16)
    slot_rows = lax.broadcasted_iota(jnp.int32, (total_rows, ep_count), 0)
    slot_experts = lax.broadcasted_iota(jnp.int32, (total_rows, ep_count), 1)
    spread = jnp.where(slot_rows // cap == slot_experts, 1.0, 0.0).astype(bf16)
    slot_of_row = lax.broadcasted_iota(jnp.int32, (total_rows, seq_count), 0) % cap
    hits = jnp.dot(spread, slots, preferred_element_type=f32) == slot_of_row.astype(f32)
    chooser = jnp.where(hits, 1.0, 0.0)
    place_own[...] = chooser.astype(bf16).reshape(n_groups, block_rows, seq_count)
    place_all[group] = place_own[group]

    def across(block, source, target, send_sems, recv_sems):
        return remote(
            source,
            target.at[group],
            send_sems.at[block],
            recv_sems.at[group],
            (target_group(block) * size + rank, core),
        )

    def across_arrival(block, source, target, send_sems, recv_sems):
        origin = source_group(block)
        return remote(
            source,
            target.at[origin],
            send_sems.at[block],
            recv_sems.at[origin],
            (origin * size + rank, core),
        )

    def place_args(block):
        return (block, place_own.at[target_group(block)], place_all, place_send_sems, place_recv_sems)

    def comb_args(block):
        return (block, comb_own.at[target_group(block)], comb_all, comb_send_sems, comb_recv_sems)

    def cross_args(block):
        return (block, rows_own, rows_all, cross_send_sems, cross_recv_sems)

    def sum_args(block):
        return (block, total_send.at[block], total_recv, total_send_sems, total_recv_sems)

    def fan_copy(block, step):
        return remote(
            send_buf.at[block, to_rank[step]],
            rows_buf.at[block, rank],
            fan_send_sems.at[block, step],
            fan_recv_sems.at[block, rank],
            (base + to_rank[step], core),
        )

    def fan_arrival(block, step):
        return remote(
            send_buf.at[block, to_rank[step]],
            rows_buf.at[block, from_rank[step]],
            fan_send_sems.at[block, step],
            fan_recv_sems.at[block, from_rank[step]],
            (base + from_rank[step], core),
        )

    def fan_out(block):
        origin = source_group(block)
        rows = jnp.dot(place_all[origin], rows_all[origin], preferred_element_type=f32)
        send_buf[block] = rows.astype(bf16).reshape(size, cap, half)
        rows_buf[block, rank] = send_buf[block, rank]

    def fan_start(block, chosen):
        for step in chosen:
            fan_copy(block, step).start()

    for load in state_loads:
        load.start()

    for load in small[2:5]:
        load.wait()
    tokens = tokens_ref[...].astype(f32)
    factor = lax.rsqrt(jnp.mean(tokens * tokens, axis=1, keepdims=True) + 1e-06)
    normed = (tokens * factor * norm_mix_ref[...].reshape(1, width).astype(f32)).astype(bf16)
    decay_low = jnp.tanh(
        lax.dot_general(normed, decay_down_ref[...], rows_dims, preferred_element_type=f32)
    ).astype(bf16)
    iclr_low = lax.dot_general(
        normed, iclr_down_ref[...], rows_dims, preferred_element_type=f32
    ).astype(bf16)
    for load in small[5:]:
        load.wait()
    decay_in = decay_base_ref[...].reshape(1, channels) + jnp.dot(
        decay_low, decay_up_ref[...], preferred_element_type=f32
    )
    decays = jnp.exp(-jnp.exp(jnp.float32(-0.5)) * jax.nn.sigmoid(decay_in))
    rate = jax.nn.sigmoid(
        iclr_base_ref[...].reshape(1, channels)
        + jnp.dot(iclr_low, iclr_up_ref[...], preferred_element_type=f32)
    )

    def project(index):
        weight_loads[index].wait()
        rows = jnp.dot(normed, weights[index], preferred_element_type=f32)
        return rows.astype(bf16).astype(f32)

    key = project(0)
    scaled = key * key_scale_ref[...].reshape(1, channels).astype(f32)
    key_mod = key * (1.0 + (rate - 1.0) * key_mix_ref[...].reshape(1, channels).astype(f32))
    spans = [slice(head * head_size, (head + 1) * head_size) for head in range(heads)]
    units = []
    for span in spans:
        part = scaled[:, span]
        units.append(part * lax.rsqrt(jnp.sum(part * part, axis=1, keepdims=True) + 1e-06))
    recept = project(1)
    readers, writers, gains = [], [], []
    for head, span in enumerate(spans):
        unit, query = units[head], recept[:, span]
        drop = unit * rate[:, span]
        shift = jnp.sum(drop * query, axis=1, keepdims=True)
        gains.append(jnp.sum(key_mod[:, span] * query, axis=1, keepdims=True))
        reader = decays[:, span] * query - unit * shift
        readers.append(jnp.concatenate([unit, reader], axis=0).astype(bf16))
        writers.append(jnp.concatenate([-drop, key_mod[:, span]], axis=0).astype(bf16))
    value = project(2)
    value_t = jnp.concatenate([value, value], axis=0).T
    for load in loads:
        load.start()
    pl.semaphore_wait(barrier, (n_groups - 1) + (size - 1) + 1)
    for share in shares:
        share.start()
    each(1, n_groups, lambda block: across(*place_args(block)).start())

    def relay_rows(block):
        across_arrival(*cross_args(block)).wait_recv()
        across_arrival(*place_args(block)).wait_recv()
        fan_out(block)
        fan_start(block, steps)

    lanes = lax.broadcasted_iota(jnp.int32, (per_chunk, head_size, 2 * seq_count), 2)
    seqs = lax.broadcasted_iota(jnp.int32, (per_chunk, head_size, 2 * seq_count), 0)
    first = lanes < seq_count
    owner = jnp.where(first, lanes, lanes - seq_count)
    totals = [jnp.zeros((head_size, 2 * seq_count), f32) for _ in range(heads)]
    for index in range(n_chunks):
        rows = slice(index * per_chunk, (index + 1) * per_chunk)
        here = owner == seqs + index * per_chunk
        state_loads[index].wait()
        for head, span in enumerate(spans):
            flat = state_buf[rows, head].reshape(per_chunk * head_size, head_size).astype(bf16)
            read = lax.dot_general(flat, readers[head], rows_dims, preferred_element_type=f32)
            read = read.reshape(per_chunk, head_size, 2 * seq_count)
            totals[head] += jnp.sum(jnp.where(here, read, 0.0), axis=0)
            terms = jnp.where(here, jnp.where(first, read, value_t[span, :][None]), 0.0)
            terms_buf[head, rows] = terms.astype(bf16)
    total = jnp.concatenate(totals, axis=0).T[seq_count:]
    mixed = [total[:, span] + value[:, span] * gains[head] for head, span in enumerate(spans)]
    mixed = jnp.concatenate(mixed, axis=1).astype(bf16)
    for head, span in enumerate(spans):
        decay_buf[head] = decays[:, span]
        writer_buf[head] = writers[head]

    loads[0].wait()
    for index in range(2):
        columns = slice(index * half, (index + 1) * half)
        part_buf[index] = jnp.dot(mixed, w_out_ref[:, columns], preferred_element_type=f32)
    part_copy = remote(part_buf, part_recv, part_sems.at[0], part_sems.at[1], partner)
    part_copy.start()

    def update_state():
        for index in range(n_chunks):
            rows = slice(index * per_chunk, (index + 1) * per_chunk)
            for head in range(heads):
                terms = terms_buf[head, rows].reshape(per_chunk * head_size, 2 * seq_count)
                change = jnp.dot(terms, writer_buf[head], preferred_element_type=f32)
                state_out_ref[rows, head] = state_buf[rows, head] * decay_buf[head, rows][
                    :, None, :
                ] + change.reshape(per_chunk, head_size, head_size)

    part_copy.wait()

    squares = jnp.zeros((seq_count, 1), f32)
    for index in range(2):
        columns = slice(index * half, (index + 1) * half)
        mixer_out = (part_buf[index] + part_recv[index]).astype(bf16)
        mid = (tokens_ref[:, columns].astype(f32) + mixer_out.astype(f32)).astype(bf16)
        mid_buf[index] = mid
        mid32 = mid.astype(f32)
        squares = squares + jnp.sum(mid32 * mid32, axis=1, keepdims=True)
    factor = lax.rsqrt(squares / width + 1e-06)
    for index in range(2):
        columns = slice(index * half, (index + 1) * half)
        norm_buf[index] = (
            mid_buf[index].astype(f32) * factor * norm_ref[columns].reshape(1, half).astype(f32)
        ).astype(bf16)
    rows_own[...] = norm_buf[core]
    each(1, n_groups, lambda block: across(*cross_args(block)).start())
    rows_all[group] = rows_own[...]
    fan_out(0)
    fan_start(0, steps)
    group_logit = jnp.zeros(group_hit.shape, f32)
    expert_logit = jnp.zeros(uses.shape, f32)
    for index in range(2):
        columns = slice(index * half, (index + 1) * half)
        group_logit += lax.dot_general(
            router_group_ref[:, columns], norm_buf[index], rows_dims, preferred_element_type=f32
        )
        expert_logit += lax.dot_general(
            router_expert_ref[:, columns], norm_buf[index], rows_dims, preferred_element_type=f32
        )
    group_prob = jax.nn.sigmoid(jnp.sum(group_logit * group_hit, axis=0, keepdims=True))
    scores = jax.nn.sigmoid(expert_logit) * uses
    route_weights = group_prob * scores / jnp.sum(scores, axis=0, keepdims=True)
    combine = jnp.dot(spread, route_weights.astype(bf16), preferred_element_type=f32) * chooser
    combine = combine.T.astype(bf16)
    for index in range(n_groups):
        comb_own[index] = combine[:, index * block_rows : (index + 1) * block_rows]
    comb_all[group] = comb_own[group]
    each(1, n_groups, lambda block: across(*comb_args(block)).start())

    update_state()
    each(1, n_groups, relay_rows)
    for load in loads[1:]:
        load.wait()
    for share in shares:
        share.wait_recv()
    def sums_copy(block):
        return remote(
            sums_own.at[block],
            sums_recv.at[block],
            sums_send_sems.at[block],
            sums_recv_sems.at[block],
            partner,
        )

    def first_products(block):
        for step in reversed(steps):
            fan_arrival(block, step).wait_recv()
        rows = rows_buf[block].reshape(block_rows, half)
        for index in range(2):
            sums_own[block, :, index * hidden_width : (index + 1) * hidden_width] = jnp.dot(
                rows, first_ref[index], preferred_element_type=f32
            )
        sums_copy(block).start()

    def back_copy(block, step):
        return remote(
            result_buf.at[block, to_rank[step]],
            back_buf.at[block, rank],
            back_send_sems.at[block, step],
            back_recv_sems.at[block, rank],
            (base + to_rank[step], core),
        )

    def back_arrival(block, step):
        return remote(
            result_buf.at[block, to_rank[step]],
            back_buf.at[block, from_rank[step]],
            back_send_sems.at[block, step],
            back_recv_sems.at[block, from_rank[step]],
            (base + from_rank[step], core),
        )

    def second_product(block):
        sums_copy(block).wait_recv()
        sums = sums_own[block] + sums_recv[block]
        gate_part = sums[:, :hidden_width]
        up_part = sums[:, hidden_width:]
        hidden = (gate_part / (1.0 + jnp.exp(-gate_part)) * up_part).astype(bf16)
        result = jnp.dot(hidden, down_ref[...], preferred_element_type=f32)
        result_buf[block] = result.astype(bf16).reshape(size, cap, half)
        for step in steps:
            back_copy(block, step).start()
        back_buf[block, rank] = result_buf[block, rank]

    first_products(0)
    second_product(0)
    each(1, n_groups, first_products)
    each(1, n_groups, second_product)

    def gather(block):
        for step in reversed(steps):
            back_arrival(block, step).wait_recv()
        back = back_buf[block].reshape(block_rows, half)
        return jnp.dot(comb_all[source_group(block)], back, preferred_element_type=f32)

    def sum_copy(block):
        origin = source_group(block)
        return remote(
            total_send.at[block],
            total_recv.at[group],
            total_send_sems.at[block],
            total_recv_sems.at[group],
            (origin * size + rank, core),
        )

    def return_sum(block):
        across_arrival(*comb_args(block)).wait_recv()
        total_send[block] = gather(block).astype(bf16)
        sum_copy(block).start()

    each(1, n_groups, return_sum)
    part_buf[0] = mid_buf[core].astype(f32) + gather(0)

    def add_sum(block):
        across_arrival(*sum_args(block)).wait_recv()
        part_buf[0] += total_recv[source_group(block)].astype(f32)

    each(1, n_groups, add_sum)
    out_ref[...] = part_buf[0].astype(bf16)

    def finish_block(block):
        for step in steps:
            fan_copy(block, step).wait_send()
            back_copy(block, step).wait_send()
        sums_copy(block).wait_send()

    each(0, n_groups, finish_block)

    def finish_cross(block):
        across(*place_args(block)).wait_send()
        across(*cross_args(block)).wait_send()
        across(*comb_args(block)).wait_send()
        sum_copy(block).wait_send()

    each(1, n_groups, finish_cross)
    for share in shares:
        share.wait_send()


def shards(
    tokens_in,
    state_in,
    norm_mix,
    w_recept,
    w_key,
    w_value,
    decay_down,
    decay_up,
    decay_base,
    iclr_down,
    iclr_up,
    iclr_base,
    key_scale,
    key_mix,
    w_out,
    norm_moe,
    router_group,
    router_expert,
    routes,
    expert_gate,
    expert_up,
    expert_down,
):
    f32 = jnp.float32
    bf16 = jnp.bfloat16
    seq_count, width_model = tokens_in.shape
    heads_here, head_size = state_in.shape[1], state_in.shape[3]
    channels = heads_here * head_size
    tp_count = lax.axis_size("tp")
    ep_count = lax.axis_size("ep")
    dma = pltpu.SemaphoreType.DMA
    vmem = pl.BlockSpec(memory_space=pltpu.VMEM)
    anywhere = pl.BlockSpec(memory_space=pl.ANY)
    n_chunks = 2 if seq_count % 2 == 0 else 1
    top_count = routes.shape[1]
    half_width = width_model // tp_count
    limit = max(2, 2 * seq_count * top_count // ep_count)
    cap = -(-limit // 16) * 16
    n_groups = router_group.shape[1]
    size = ep_count // n_groups
    block_rows = size * cap
    hidden_width = expert_gate.shape[2]
    block_bytes = ep_count * cap * width_model
    vmem_limit = min(58 * 1024 * 1024, 24 * 1024 * 1024 + 10 * block_bytes)
    vmem_of = pltpu.VMEM
    small = (
        tokens_in, routes.T, norm_mix, decay_down.T, iclr_down.T, decay_up, decay_base,
        iclr_up, iclr_base, key_scale, key_mix, norm_moe, router_group.T, router_expert.T,
    )
    large = (
        w_recept, w_key, w_value, state_in, w_out, expert_gate, expert_up, expert_down,
    )
    operands = small + large
    layer = pl.pallas_call(
        functools.partial(layer_kernel, ep_count),
        out_shape=(
            jax.ShapeDtypeStruct((seq_count, half_width), bf16),
            jax.ShapeDtypeStruct(state_in.shape, f32),
        ),
        in_specs=[anywhere] * len(operands),
        out_specs=(vmem, vmem),
        scratch_shapes=[vmem_of(operand.shape, operand.dtype) for operand in small]
        + [
            vmem_of((3, width_model, channels), bf16),
            vmem_of(state_in.shape, f32),
            vmem_of((heads_here, seq_count, head_size, 2 * seq_count), bf16),
            vmem_of((heads_here, seq_count, head_size), f32),
            vmem_of((heads_here, 2 * seq_count, head_size), bf16),
            vmem_of(w_out.shape, bf16),
            vmem_of((2, half_width, tp_count * hidden_width), bf16),
            vmem_of((tp_count * hidden_width, half_width), bf16),
            vmem_of((tp_count, seq_count, half_width), f32),
            vmem_of((tp_count, seq_count, half_width), f32),
            vmem_of((tp_count, seq_count, half_width), bf16),
            vmem_of((tp_count, seq_count, half_width), bf16),
            vmem_of((n_groups, block_rows, seq_count), bf16),
            vmem_of((n_groups, block_rows, seq_count), bf16),
            vmem_of((n_groups, seq_count, block_rows), bf16),
            vmem_of((n_groups, seq_count, block_rows), bf16),
            vmem_of((seq_count, half_width), bf16),
            vmem_of((n_groups, seq_count, half_width), bf16),
            vmem_of((n_groups, size, cap, half_width), bf16),
            vmem_of((n_groups, size, cap, half_width), bf16),
            vmem_of((n_groups, block_rows, 2 * tp_count * hidden_width), f32),
            vmem_of((n_groups, block_rows, 2 * tp_count * hidden_width), f32),
            vmem_of((n_groups, size, cap, half_width), bf16),
            vmem_of((n_groups, size, cap, half_width), bf16),
            vmem_of((n_groups, seq_count, half_width), bf16),
            vmem_of((n_groups, seq_count, half_width), bf16),
            dma((len(small),)),
            dma((3,)),
            dma((n_chunks,)),
            dma((4,)),
            dma((3,)),
            dma((3,)),
            dma((2,)),
            dma((n_groups,)),
            dma((n_groups,)),
            dma((n_groups,)),
            dma((n_groups,)),
            dma((n_groups,)),
            dma((n_groups,)),
            dma((n_groups, size)),
            dma((n_groups, size)),
            dma((n_groups,)),
            dma((n_groups,)),
            dma((n_groups, size)),
            dma((n_groups, size)),
            dma((n_groups,)),
            dma((n_groups,)),
        ],
        compiler_params=pltpu.CompilerParams(
            collective_id=0, has_side_effects=True, vmem_limit_bytes=vmem_limit
        ),
    )
    layer_out, state_out = layer(
        *(pltpu.with_memory_space_constraint(operand, pltpu.HBM) for operand in operands)
    )
    return (layer_out, state_out)


def solution(mesh):
    in_specs = (
        P("ep", None),
        P("ep", "tp", None, None),
        P(),
        P(None, "tp"),
        P(None, "tp"),
        P(None, "tp"),
        P(),
        P(None, "tp"),
        P("tp"),
        P(),
        P(None, "tp"),
        P("tp"),
        P("tp"),
        P("tp"),
        P("tp", None),
        P(),
        P(),
        P(),
        P("ep", None),
        P("ep", None, "tp"),
        P("ep", None, "tp"),
        P("ep", "tp", None),
    )
    out_specs = (P("ep", "tp"), P("ep", "tp", None, None))
    return jax.shard_map(shards, mesh=mesh, in_specs=in_specs, out_specs=out_specs, check_vma=False)
```

time: 39.3 us -> 36.5 us (0.929)
  Pallas kernels: 35.9 us -> 33 us
    pallas_call x1, Pallas kernels: 35.9 us -> 33 us  [shards(): layer(*(pltpu.with_memory_space_constraint(operand, pltpu.HBM) for operan...]
where the time goes in v4:
time: 36.5 us; the launch traced here: 36.3 us
  Pallas kernels  33 us (90%)
  local copies, waits for them, and re-layouts  2.64 us (7%)
  between operations  0.65 us (2%)
    pallas_call x1, Pallas kernels, shards(): layer(*(pltpu.with_memory_space_constraint(operand, pltpu.HBM) for operan...  33 us
    unnamed x2, local copies, waits for them, and re-layouts  2.64 us

profile of v4, /device:TPU:0, one launch (start us, length us, event | category | flops | bytes accessed | tf_op | source)
XLA Modules:
  0.0 36.3 jit_solution(8174806699650297598)
XLA Ops:
  0.6 33.0 %shard_map.221 = (bf16[32,1024]{1,0:T(8,128)(2,1)S(1)}, f32[32,4,64,64]{3,2,1,0:T(8,128)S(1)}) custom-call(bf16[32,2048]{1,0:T(8,128)(2,1)} %tokens_hbm.1, s32[4,32]{1,0:T(4,128)} %bitcast.9, bf16[2048]{0:T(1024)(128)(2,1)} %norm_mix_hbm.1, bf16[64,2048]{1,0:T(8,128)(2,1)} %bitcast.5, bf16[64,2048]{1,0:T(8,128)(2,1)} %bitcast.6, ...), custom_call_target="tpu_custom_call" | custom-call | tf_op jit(solution)/shard_map/pallas_call | solution.py:679
  33.7 0.6 %copy.26 = bf16[32,1024]{1,0:T(8,128)(2,1)} copy(bf16[32,1024]{1,0:T(8,128)(2,1)S(1)} %get-tuple-element.4) | data formatting | bytes 131072
  34.3 2.0 %copy.27 = f32[32,4,64,64]{3,2,1,0:T(8,128)} copy(f32[32,4,64,64]{3,2,1,0:T(8,128)S(1)} %get-tuple-element.5) | data formatting | bytes 4194304

commit v5 on v4

--- a/solution.py
+++ b/solution.py
@@ -53,18 +53,20 @@
     terms_buf,
     decay_buf,
     writer_buf,
-    w_out_ref,
+    w_cols,
     first_ref,
     down_ref,
-    part_buf,
-    part_recv,
-    mid_buf,
-    norm_buf,
+    final_buf,
+    logit_own,
+    logit_recv,
     place_own,
     place_all,
     comb_own,
     comb_all,
-    rows_own,
+    tokens_own,
+    tokens_all,
+    mix_own,
+    mix_all,
     rows_all,
     send_buf,
     rows_buf,
@@ -80,13 +82,15 @@
     load_sems,
     share_send_sems,
     share_recv_sems,
-    part_sems,
+    logit_sems,
     place_send_sems,
     place_recv_sems,
     comb_send_sems,
     comb_recv_sems,
     cross_send_sems,
     cross_recv_sems,
+    mix_send_sems,
+    mix_recv_sems,
     fan_send_sems,
     fan_recv_sems,
     sums_send_sems,
@@ -158,12 +162,14 @@
         )
 
     partner = (me, other)
+    pieces = (slice(0, half // 2), slice(half // 2, half))
     barrier = pltpu.get_barrier_semaphore()
 
     def greet(device):
         pl.semaphore_signal(barrier, inc=1, device_id=device, device_id_type=mesh_ids)
 
-    each(1, n_groups, lambda block: greet((target_group(block) * size + rank, core)))
+    for which in (core, other):
+        each(1, n_groups, lambda block: greet((target_group(block) * size + rank, which)))
     for step in steps:
         greet((base + to_rank[step], core))
     greet(partner)
@@ -211,14 +217,15 @@
 
     hidden_here = pl.ds(pl.multiple_of(core * hidden_part, hidden_part), hidden_part)
     shared = (
+        (lambda which: w_out_hbm.at[:, columns_of(which)], w_cols.at[core]),
         (lambda which: gate_hbm.at[0, columns_of(which)], first_ref.at[0, :, hidden_here]),
         (lambda which: up_hbm.at[0, columns_of(which)], first_ref.at[1, :, hidden_here]),
         (lambda which: down_hbm.at[0, :, columns_of(which)], down_ref.at[hidden_here]),
     )
-    loads = [pltpu.make_async_copy(w_out_hbm, w_out_ref, load_sems.at[0])]
+    loads = []
     shares = []
     for index, (source, target) in enumerate(shared):
-        loads.append(pltpu.make_async_copy(source(core), target, load_sems.at[1 + index]))
+        loads.append(pltpu.make_async_copy(source(core), target, load_sems.at[index]))
         shares.append(
             remote(
                 source(other), target, share_send_sems.at[index], share_recv_sems.at[index], partner
@@ -246,6 +253,8 @@
     chooser = jnp.where(hits, 1.0, 0.0)
     place_own[...] = chooser.astype(bf16).reshape(n_groups, block_rows, seq_count)
     place_all[group] = place_own[group]
+    tokens_own[...] = jnp.where(core == 0, tokens_ref[:, :half], tokens_ref[:, half:])
+    tokens_all[group] = tokens_own[...]
 
     def across(block, source, target, send_sems, recv_sems):
         return remote(
@@ -273,10 +282,27 @@
         return (block, comb_own.at[target_group(block)], comb_all, comb_send_sems, comb_recv_sems)
 
     def cross_args(block):
-        return (block, rows_own, rows_all, cross_send_sems, cross_recv_sems)
-
-    def sum_args(block):
-        return (block, total_send.at[block], total_recv, total_send_sems, total_recv_sems)
+        return (block, tokens_own, tokens_all, cross_send_sems, cross_recv_sems)
+
+    def mix_copy(block, index):
+        return remote(
+            mix_own,
+            mix_all.at[group, core],
+            mix_send_sems.at[block, index],
+            mix_recv_sems.at[group, core],
+            (target_group(block) * size + rank, (core, other)[index]),
+        )
+
+    def mix_arrival(block, index):
+        origin = source_group(block)
+        which = (core, other)[index]
+        return remote(
+            mix_own,
+            mix_all.at[origin, which],
+            mix_send_sems.at[block, index],
+            mix_recv_sems.at[origin, which],
+            (origin * size + rank, which),
+        )
 
     def fan_copy(block, step):
         return remote(
@@ -308,6 +334,11 @@
 
     for load in state_loads:
         load.start()
+    pl.semaphore_wait(barrier, 2 * (n_groups - 1) + (size - 1) + 1)
+    loads[0].start()
+    shares[0].start()
+    each(1, n_groups, lambda block: across(*cross_args(block)).start())
+    each(1, n_groups, lambda block: across(*place_args(block)).start())
 
     for load in small[2:5]:
         load.wait()
@@ -356,16 +387,24 @@
         writers.append(jnp.concatenate([-drop, key_mod[:, span]], axis=0).astype(bf16))
     value = project(2)
     value_t = jnp.concatenate([value, value], axis=0).T
-    for load in loads:
+    for load in loads[1:]:
         load.start()
-    pl.semaphore_wait(barrier, (n_groups - 1) + (size - 1) + 1)
-    for share in shares:
-        share.start()
-    each(1, n_groups, lambda block: across(*place_args(block)).start())
+
+    def make_rows(origin):
+        mixer_out = jnp.zeros((seq_count, half), f32)
+        for index in range(2):
+            mixer_out += jnp.dot(
+                mix_all[origin, index], w_cols[index], preferred_element_type=f32
+            )
+        mid = tokens_all[origin].astype(f32) + mixer_out.astype(bf16).astype(f32)
+        rows_all[origin] = mid.astype(bf16)
 
     def relay_rows(block):
         across_arrival(*cross_args(block)).wait_recv()
         across_arrival(*place_args(block)).wait_recv()
+        for index in range(2):
+            mix_arrival(block, index).wait_recv()
+        make_rows(source_group(block))
         fan_out(block)
         fan_start(block, steps)
 
@@ -392,13 +431,6 @@
         decay_buf[head] = decays[:, span]
         writer_buf[head] = writers[head]
 
-    loads[0].wait()
-    for index in range(2):
-        columns = slice(index * half, (index + 1) * half)
-        part_buf[index] = jnp.dot(mixed, w_out_ref[:, columns], preferred_element_type=f32)
-    part_copy = remote(part_buf, part_recv, part_sems.at[0], part_sems.at[1], partner)
-    part_copy.start()
-
     def update_state():
         for index in range(n_chunks):
             rows = slice(index * per_chunk, (index + 1) * per_chunk)
@@ -409,37 +441,45 @@
                     :, None, :
                 ] + change.reshape(per_chunk, head_size, head_size)
 
-    part_copy.wait()
-
-    squares = jnp.zeros((seq_count, 1), f32)
-    for index in range(2):
-        columns = slice(index * half, (index + 1) * half)
-        mixer_out = (part_buf[index] + part_recv[index]).astype(bf16)
-        mid = (tokens_ref[:, columns].astype(f32) + mixer_out.astype(f32)).astype(bf16)
-        mid_buf[index] = mid
-        mid32 = mid.astype(f32)
-        squares = squares + jnp.sum(mid32 * mid32, axis=1, keepdims=True)
-    factor = lax.rsqrt(squares / width + 1e-06)
-    for index in range(2):
-        columns = slice(index * half, (index + 1) * half)
-        norm_buf[index] = (
-            mid_buf[index].astype(f32) * factor * norm_ref[columns].reshape(1, half).astype(f32)
-        ).astype(bf16)
-    rows_own[...] = norm_buf[core]
-    each(1, n_groups, lambda block: across(*cross_args(block)).start())
-    rows_all[group] = rows_own[...]
+    mix_own[...] = mixed
+
+    def send_mixed(block):
+        for index in range(2):
+            mix_copy(block, index).start()
+
+    each(1, n_groups, send_mixed)
+    mix_copy(0, 1).start()
+    mix_all[group, core] = mix_own[...]
+    loads[0].wait()
+    shares[0].wait_recv()
+    mix_arrival(0, 1).wait_recv()
+    make_rows(group)
     fan_out(0)
     fan_start(0, steps)
-    group_logit = jnp.zeros(group_hit.shape, f32)
-    expert_logit = jnp.zeros(uses.shape, f32)
-    for index in range(2):
-        columns = slice(index * half, (index + 1) * half)
-        group_logit += lax.dot_general(
-            router_group_ref[:, columns], norm_buf[index], rows_dims, preferred_element_type=f32
-        )
-        expert_logit += lax.dot_general(
-            router_expert_ref[:, columns], norm_buf[index], rows_dims, preferred_element_type=f32
-        )
+
+    norm_here = jnp.where(core == 0, norm_ref[:half].reshape(1, half), norm_ref[half:].reshape(1, half))
+    norm_here = norm_here.astype(f32)
+    mid = rows_all[group].astype(f32)
+    squares = jnp.sum(mid * mid, axis=1, keepdims=True)
+    normed = (mid * norm_here).astype(bf16)
+    for router, row in ((router_expert_ref, 0), (router_group_ref, ep_count)):
+        columns = jnp.where(core == 0, router[:, :half], router[:, half:])
+        logit_own[row : row + router.shape[0], :] = lax.dot_general(
+            columns, normed, rows_dims, preferred_element_type=f32
+        )
+    last = ep_count + n_groups
+    logit_own[last : last + 1, :] = jnp.broadcast_to(squares, (seq_count, 128)).T[:1]
+    logit_copy = remote(logit_own, logit_recv, logit_sems.at[0], logit_sems.at[1], partner)
+    logit_copy.start()
+    each(1, n_groups, relay_rows)
+    for share in shares[1:]:
+        share.start()
+    update_state()
+    logit_copy.wait_recv()
+    logits = logit_own[...] + logit_recv[...]
+    logits = logits * lax.rsqrt(logits[last : last + 1] / width + 1e-06)
+    expert_logit = logits[:ep_count]
+    group_logit = logits[ep_count:last]
     group_prob = jax.nn.sigmoid(jnp.sum(group_logit * group_hit, axis=0, keepdims=True))
     scores = jax.nn.sigmoid(expert_logit) * uses
     route_weights = group_prob * scores / jnp.sum(scores, axis=0, keepdims=True)
@@ -450,11 +490,9 @@
     comb_all[group] = comb_own[group]
     each(1, n_groups, lambda block: across(*comb_args(block)).start())
 
-    update_state()
-    each(1, n_groups, relay_rows)
     for load in loads[1:]:
         load.wait()
-    for share in shares:
+    for share in shares[1:]:
         share.wait_recv()
     def sums_copy(block):
         return remote(
@@ -468,83 +506,103 @@
     def first_products(block):
         for step in reversed(steps):
             fan_arrival(block, step).wait_recv()
-        rows = rows_buf[block].reshape(block_rows, half)
+        rows = rows_buf[block].reshape(block_rows, half).astype(f32)
+        squares = jnp.sum(rows * rows, axis=1, keepdims=True)
+        rows = (rows * norm_here).astype(bf16)
         for index in range(2):
             sums_own[block, :, index * hidden_width : (index + 1) * hidden_width] = jnp.dot(
                 rows, first_ref[index], preferred_element_type=f32
             )
+        tail = sums_own.shape[2] - 2 * hidden_width
+        sums_own[block, :, 2 * hidden_width :] = jnp.broadcast_to(squares, (block_rows, tail))
         sums_copy(block).start()
 
-    def back_copy(block, step):
-        return remote(
-            result_buf.at[block, to_rank[step]],
-            back_buf.at[block, rank],
-            back_send_sems.at[block, step],
-            back_recv_sems.at[block, rank],
+    def back_copy(block, step, piece):
+        return remote(
+            result_buf.at[piece, block, to_rank[step]],
+            back_buf.at[piece, block, rank],
+            back_send_sems.at[piece, block, step],
+            back_recv_sems.at[piece, block, rank],
             (base + to_rank[step], core),
         )
 
-    def back_arrival(block, step):
-        return remote(
-            result_buf.at[block, to_rank[step]],
-            back_buf.at[block, from_rank[step]],
-            back_send_sems.at[block, step],
-            back_recv_sems.at[block, from_rank[step]],
+    def back_arrival(block, step, piece):
+        return remote(
+            result_buf.at[piece, block, to_rank[step]],
+            back_buf.at[piece, block, from_rank[step]],
+            back_send_sems.at[piece, block, step],
+            back_recv_sems.at[piece, block, from_rank[step]],
             (base + from_rank[step], core),
         )
 
     def second_product(block):
         sums_copy(block).wait_recv()
         sums = sums_own[block] + sums_recv[block]
-        gate_part = sums[:, :hidden_width]
-        up_part = sums[:, hidden_width:]
+        factor = lax.rsqrt(sums[:, 2 * hidden_width : 2 * hidden_width + 1] / width + 1e-06)
+        gate_part = sums[:, :hidden_width] * factor
+        up_part = sums[:, hidden_width : 2 * hidden_width] * factor
         hidden = (gate_part / (1.0 + jnp.exp(-gate_part)) * up_part).astype(bf16)
-        result = jnp.dot(hidden, down_ref[...], preferred_element_type=f32)
-        result_buf[block] = result.astype(bf16).reshape(size, cap, half)
-        for step in steps:
-            back_copy(block, step).start()
-        back_buf[block, rank] = result_buf[block, rank]
+        for piece in range(2):
+            result = jnp.dot(hidden, down_ref[:, pieces[piece]], preferred_element_type=f32)
+            result_buf[piece, block] = result.astype(bf16).reshape(size, cap, half // 2)
+            for step in steps:
+                back_copy(block, step, piece).start()
+            back_buf[piece, block, rank] = result_buf[piece, block, rank]
 
     first_products(0)
     second_product(0)
     each(1, n_groups, first_products)
     each(1, n_groups, second_product)
 
-    def gather(block):
+    def gather(block, piece):
         for step in reversed(steps):
-            back_arrival(block, step).wait_recv()
-        back = back_buf[block].reshape(block_rows, half)
+            back_arrival(block, step, piece).wait_recv()
+        back = back_buf[piece, block].reshape(block_rows, half // 2)
         return jnp.dot(comb_all[source_group(block)], back, preferred_element_type=f32)
 
-    def sum_copy(block):
+    def sum_copy(block, piece):
         origin = source_group(block)
         return remote(
-            total_send.at[block],
-            total_recv.at[group],
-            total_send_sems.at[block],
-            total_recv_sems.at[group],
+            total_send.at[piece, block],
+            total_recv.at[piece, group],
+            total_send_sems.at[piece, block],
+            total_recv_sems.at[piece, group],
+            (origin * size + rank, core),
+        )
+
+    def sum_arrival(block, piece):
+        origin = source_group(block)
+        return remote(
+            total_send.at[piece, block],
+            total_recv.at[piece, origin],
+            total_send_sems.at[piece, block],
+            total_recv_sems.at[piece, origin],
             (origin * size + rank, core),
         )
 
     def return_sum(block):
         across_arrival(*comb_args(block)).wait_recv()
-        total_send[block] = gather(block).astype(bf16)
-        sum_copy(block).start()
+        for piece in range(2):
+            total_send[piece, block] = gather(block, piece).astype(bf16)
+            sum_copy(block, piece).start()
 
     each(1, n_groups, return_sum)
-    part_buf[0] = mid_buf[core].astype(f32) + gather(0)
+    for piece, columns in enumerate(pieces):
+        final_buf[:, columns] = rows_all[group, :, columns].astype(f32) + gather(0, piece)
 
     def add_sum(block):
-        across_arrival(*sum_args(block)).wait_recv()
-        part_buf[0] += total_recv[source_group(block)].astype(f32)
+        for piece, columns in enumerate(pieces):
+            sum_arrival(block, piece).wait_recv()
+            final_buf[:, columns] += total_recv[piece, source_group(block)].astype(f32)
 
     each(1, n_groups, add_sum)
-    out_ref[...] = part_buf[0].astype(bf16)
+    out_ref[...] = final_buf[...].astype(bf16)
 
     def finish_block(block):
         for step in steps:
             fan_copy(block, step).wait_send()
-            back_copy(block, step).wait_send()
+            for piece in range(2):
+                back_copy(block, step, piece).wait_send()
         sums_copy(block).wait_send()
 
     each(0, n_groups, finish_block)
@@ -552,12 +610,32 @@
     def finish_cross(block):
         across(*place_args(block)).wait_send()
         across(*cross_args(block)).wait_send()
+        for index in range(2):
+            mix_copy(block, index).wait_send()
         across(*comb_args(block)).wait_send()
-        sum_copy(block).wait_send()
+        for piece in range(2):
+            sum_copy(block, piece).wait_send()
 
     each(1, n_groups, finish_cross)
     for share in shares:
         share.wait_send()
+    mix_copy(0, 1).wait_send()
+    logit_copy.wait_send()
+
+
+def store_kernel(out_vmem, state_vmem, out_hbm, state_hbm, sems):
+    n_chunks = sems.shape[0] - 1
+    per_chunk = state_hbm.shape[0] // n_chunks
+    copies = [pltpu.make_async_copy(out_vmem, out_hbm, sems.at[n_chunks])]
+    for index in range(n_chunks):
+        span = pl.ds(index * per_chunk, per_chunk)
+        copies.append(
+            pltpu.make_async_copy(state_vmem.at[span], state_hbm.at[span], sems.at[index])
+        )
+    for copy in copies:
+        copy.start()
+    for copy in copies:
+        copy.wait()
 
 
 def shards(
@@ -629,33 +707,35 @@
             vmem_of((heads_here, seq_count, head_size, 2 * seq_count), bf16),
             vmem_of((heads_here, seq_count, head_size), f32),
             vmem_of((heads_here, 2 * seq_count, head_size), bf16),
-            vmem_of(w_out.shape, bf16),
+            vmem_of((tp_count, channels, half_width), bf16),
             vmem_of((2, half_width, tp_count * hidden_width), bf16),
             vmem_of((tp_count * hidden_width, half_width), bf16),
-            vmem_of((tp_count, seq_count, half_width), f32),
-            vmem_of((tp_count, seq_count, half_width), f32),
-            vmem_of((tp_count, seq_count, half_width), bf16),
-            vmem_of((tp_count, seq_count, half_width), bf16),
+            vmem_of((seq_count, half_width), f32),
+            vmem_of((ep_count + n_groups + 1, seq_count), f32),
+            vmem_of((ep_count + n_groups + 1, seq_count), f32),
             vmem_of((n_groups, block_rows, seq_count), bf16),
             vmem_of((n_groups, block_rows, seq_count), bf16),
             vmem_of((n_groups, seq_count, block_rows), bf16),
             vmem_of((n_groups, seq_count, block_rows), bf16),
             vmem_of((seq_count, half_width), bf16),
             vmem_of((n_groups, seq_count, half_width), bf16),
+            vmem_of((seq_count, channels), bf16),
+            vmem_of((n_groups, tp_count, seq_count, channels), bf16),
+            vmem_of((n_groups, seq_count, half_width), bf16),
             vmem_of((n_groups, size, cap, half_width), bf16),
             vmem_of((n_groups, size, cap, half_width), bf16),
-            vmem_of((n_groups, block_rows, 2 * tp_count * hidden_width), f32),
-            vmem_of((n_groups, block_rows, 2 * tp_count * hidden_width), f32),
-            vmem_of((n_groups, size, cap, half_width), bf16),
-            vmem_of((n_groups, size, cap, half_width), bf16),
-            vmem_of((n_groups, seq_count, half_width), bf16),
-            vmem_of((n_groups, seq_count, half_width), bf16),
+            vmem_of((n_groups, block_rows, 2 * tp_count * hidden_width + 128), f32),
+            vmem_of((n_groups, block_rows, 2 * tp_count * hidden_width + 128), f32),
+            vmem_of((2, n_groups, size, cap, half_width // 2), bf16),
+            vmem_of((2, n_groups, size, cap, half_width // 2), bf16),
+            vmem_of((2, n_groups, seq_count, half_width // 2), bf16),
+            vmem_of((2, n_groups, seq_count, half_width // 2), bf16),
             dma((len(small),)),
             dma((3,)),
             dma((n_chunks,)),
             dma((4,)),
-            dma((3,)),
-            dma((3,)),
+            dma((4,)),
+            dma((4,)),
             dma((2,)),
             dma((n_groups,)),
             dma((n_groups,)),
@@ -663,14 +743,16 @@
             dma((n_groups,)),
             dma((n_groups,)),
             dma((n_groups,)),
+            dma((n_groups, tp_count)),
+            dma((n_groups, tp_count)),
             dma((n_groups, size)),
             dma((n_groups, size)),
             dma((n_groups,)),
             dma((n_groups,)),
-            dma((n_groups, size)),
-            dma((n_groups, size)),
-            dma((n_groups,)),
-            dma((n_groups,)),
+            dma((2, n_groups, size)),
+            dma((2, n_groups, size)),
+            dma((2, n_groups)),
+            dma((2, n_groups)),
         ],
         compiler_params=pltpu.CompilerParams(
             collective_id=0, has_side_effects=True, vmem_limit_bytes=vmem_limit
@@ -679,7 +761,18 @@
     layer_out, state_out = layer(
         *(pltpu.with_memory_space_constraint(operand, pltpu.HBM) for operand in operands)
     )
-    return (layer_out, state_out)
+    pieces = 4 if seq_count % 4 == 0 else 1
+    return pl.pallas_call(
+        store_kernel,
+        out_shape=(
+            jax.ShapeDtypeStruct(layer_out.shape, bf16),
+            jax.ShapeDtypeStruct(state_in.shape, f32),
+        ),
+        in_specs=[vmem, vmem],
+        out_specs=(anywhere, anywhere),
+        scratch_shapes=[dma((pieces + 1,))],
+        compiler_params=pltpu.CompilerParams(vmem_limit_bytes=8 * 1024 * 1024),
+    )(layer_out, state_out)
 
 
 def solution(mesh):

time: 36.5 us -> 34.2 us (0.937)
  local copies, waits for them, and re-layouts: 2.64 us -> 0 us
  Pallas kernels: 33 us -> 33.4 us
    unnamed x2 -> x0, local copies, waits for them, and re-layouts: 2.64 us -> none
    pallas_call x0 -> x1, Pallas kernels: none -> 2.07 us  [shards(): pl.pallas_call(store_kernel, out_shape=(jax.ShapeDtypeStruct(layer_out.sh...]
    pallas_call x1, Pallas kernels: 33 us -> 31.3 us  [shards(): layer(*(pltpu.with_memory_space_constraint(operand, pltpu.HBM) for operan...]
where the time goes in v5:
time: 34.2 us; the launch traced here: 34.1 us
  Pallas kernels  33.4 us (98%)
  between operations  0.65 us (2%)
    pallas_call x1, Pallas kernels, shards(): layer(*(pltpu.with_memory_space_constraint(operand, pltpu.HBM) for operan...  31.3 us
    pallas_call x1, Pallas kernels, shards(): pl.pallas_call(store_kernel, out_shape=(jax.ShapeDtypeStruct(layer_out.sh...  2.07 us

profile of v5, /device:TPU:0, one launch (start us, length us, event | category | flops | bytes accessed | tf_op | source)
XLA Modules:
  0.0 34.1 jit_solution(839990277135749663)
XLA Ops:
  0.6 31.3 %shard_map.221 = (bf16[32,1024]{1,0:T(8,128)(2,1)S(1)}, f32[32,4,64,64]{3,2,1,0:T(8,128)S(1)}) custom-call(bf16[32,2048]{1,0:T(8,128)(2,1)} %tokens_hbm.1, s32[4,32]{1,0:T(4,128)} %bitcast.9, bf16[2048]{0:T(1024)(128)(2,1)} %norm_mix_hbm.1, bf16[64,2048]{1,0:T(8,128)(2,1)} %bitcast.5, bf16[64,2048]{1,0:T(8,128)(2,1)} %bitcast.6, ...), custom_call_target="tpu_custom_call" | custom-call | tf_op jit(solution)/shard_map/pallas_call | solution.py:761
  32.0 2.1 %shard_map.222 = (bf16[32,1024]{1,0:T(8,128)(2,1)}, f32[32,4,64,64]{3,2,1,0:T(8,128)}) custom-call(bf16[32,1024]{1,0:T(8,128)(2,1)S(1)} %get-tuple-element.4.out_vmem, f32[32,4,64,64]{3,2,1,0:T(8,128)S(1)} %get-tuple-element.5.state_vmem), custom_call_target="tpu_custom_call" | custom-call | tf_op jit(solution)/shard_map/pallas_call | solution.py:765

commit v6 on v5

--- a/solution.py
+++ b/solution.py
@@ -452,8 +452,11 @@
     mix_all[group, core] = mix_own[...]
     loads[0].wait()
     shares[0].wait_recv()
+    mixer_out = jnp.dot(mixed, w_cols[core], preferred_element_type=f32)
     mix_arrival(0, 1).wait_recv()
-    make_rows(group)
+    mixer_out += jnp.dot(mix_all[group, other], w_cols[other], preferred_element_type=f32)
+    mid = tokens_all[group].astype(f32) + mixer_out.astype(bf16).astype(f32)
+    rows_all[group] = mid.astype(bf16)
     fan_out(0)
     fan_start(0, steps)
 

time: 34.2 us -> 34.2 us (level)
  no operation moved by 1% of the time
where the time goes in v6:
time: 34.2 us; the launch traced here: 34.1 us
  Pallas kernels  33.4 us (98%)
  between operations  0.65 us (2%)
    pallas_call x1, Pallas kernels, shards(): layer(*(pltpu.with_memory_space_constraint(operand, pltpu.HBM) for operan...  31.3 us
    pallas_call x1, Pallas kernels, shards(): pl.pallas_call(store_kernel, out_shape=(jax.ShapeDtypeStruct(layer_out.sh...  2.07 us

profile of v6, /device:TPU:0, one launch (start us, length us, event | category | flops | bytes accessed | tf_op | source)
XLA Modules:
  0.0 34.1 jit_solution(3344148900066066031)
XLA Ops:
  0.6 31.3 %shard_map.221 = (bf16[32,1024]{1,0:T(8,128)(2,1)S(1)}, f32[32,4,64,64]{3,2,1,0:T(8,128)S(1)}) custom-call(bf16[32,2048]{1,0:T(8,128)(2,1)} %tokens_hbm.1, s32[4,32]{1,0:T(4,128)} %bitcast.9, bf16[2048]{0:T(1024)(128)(2,1)} %norm_mix_hbm.1, bf16[64,2048]{1,0:T(8,128)(2,1)} %bitcast.5, bf16[64,2048]{1,0:T(8,128)(2,1)} %bitcast.6, ...), custom_call_target="tpu_custom_call" | custom-call | tf_op jit(solution)/shard_map/pallas_call | solution.py:764
  32.0 2.1 %shard_map.222 = (bf16[32,1024]{1,0:T(8,128)(2,1)}, f32[32,4,64,64]{3,2,1,0:T(8,128)}) custom-call(bf16[32,1024]{1,0:T(8,128)(2,1)S(1)} %get-tuple-element.4.out_vmem, f32[32,4,64,64]{3,2,1,0:T(8,128)S(1)} %get-tuple-element.5.state_vmem), custom_call_target="tpu_custom_call" | custom-call | tf_op jit(solution)/shard_map/pallas_call | solution.py:768
